TPU v7x, 256 devices: a whole 4x4x8 slice. The times are simulated.
256 devices in a mesh: sp: 32 (over z, y), fs: 4 (over x), tp: 2 (over core).
Axes of the slice: x: 4, y: 4, z: 8, core: 2. Of those that a mesh axis runs over, the one named last changes fastest.
Arguments:
- tokens: bfloat16 [16384, 2048], P(('fs', 'sp'), 'tp'), parts along dimension 0, may hold values from -6 to 6
- norm_gain: float32 [2048], replicated, may hold values from 0.1 to 1.9
- w_recur_in: bfloat16 [2048, 1024], P(None, 'tp'), may hold values from -0.125 to 0.125
- conv_weight: float32 [4, 1024], P(None, 'tp'), may hold values from -3 to 3
- w_gate_decay: bfloat16 [16, 64, 64], P('tp'), may hold values from -0.75 to 0.75
- w_gate_input: bfloat16 [16, 64, 64], P('tp'), may hold values from -0.75 to 0.75
- decay_base: float32 [1024], P('tp'), may hold values from 0 to 0.01, as said below
- extra_decay: float32 [16384, 16], P(('fs', 'sp'), 'tp'), parts along dimension 0, may hold values from 0 to 1, as said below
- w_query: bfloat16 [2048, 1024], P(None, 'tp'), may hold values from -1 to 1
- w_key: bfloat16 [2048, 256], P(None, 'tp'), may hold values from -20 to 20
- w_value: bfloat16 [2048, 256], P(None, 'tp'), may hold values from -0.125 to 0.125
- mix_lambda: float32 [8], P('tp'), may hold values from 0.3 to 0.8
- head_gain: float32 [128], replicated, may hold values from 0.1 to 1.9
- w_out_recur: bfloat16 [1024, 2048], P('tp'), may hold values from -0.125 to 0.125
- w_out_attend: bfloat16 [1024, 2048], P('tp'), may hold values from -0.125 to 0.125
- out_gain: float32 [2048], replicated, may hold values from 0.1 to 1.9
Outputs:
- mixed: bfloat16 [16384, 2048], P(('fs', 'sp', 'tp')), parts along dimension 0
There are 4 independent parts, one for each index of `fs`. A program takes and returns all parts, laid end to end along the dimension named above; an argument that names none is the same for every part. Nothing has to cross between parts.
Inputs may be any that keep to these rules, and one draw needn't show every extreme that they name: `decay_base`: positive rates of each channel. `extra_decay`: non-negative added log-decays.
All inputs are finite; a program needn't handle non-finite values.
Results may differ from a plain program's by a relative error of at most 0.012.
The roundings to bfloat16 on the way count: a program that leaves them out, or rounds other values in their place, can miss the bound.
Values may be sent and summed in bfloat16 or wider, within the bound.
A program may use at most 128 MiB of HBM per device.

v0:
```python
import jax
import jax.numpy as jnp
from jax import lax
from jax.sharding import PartitionSpec as P

D = 2048
HEAD = 64
DV = 128


lru_rate = 8.0
norm_eps = 1e-06


def shifted(block, axis, distance):
    devices = range(lax.axis_size(axis))
    route = [(i - distance, i) for i in devices if i - distance in devices]
    return lax.ppermute(block, axis, route)


def copy_for_each(shard, axis):
    copies = jnp.broadcast_to(shard, (lax.axis_size(axis), *shard.shape))
    return lax.all_to_all(copies, axis, split_axis=0, concat_axis=0, tiled=True)


def all_in_one(shard, axis):
    leaves = jax.tree.leaves(shard)
    sequence = sorted(range(len(leaves)), key=lambda k: -leaves[k].size)
    width = (1, *leaves[sequence[0]].shape)[-1]
    lines = [
        jnp.pad(leaves[k].reshape(-1), (0, -leaves[k].size % width)).reshape(-1, width)
        for k in sequence
    ]
    both, at, found = (copy_for_each(jnp.concatenate(lines), axis), 0, {})
    for k, line in zip(sequence, lines):
        share = both[:, at : at + len(line)].reshape(len(both), -1)
        found[k] = share[:, : leaves[k].size].reshape(-1, *leaves[k].shape)
        at += len(line)
    numbers = iter(range(len(leaves)))
    return jax.tree.map(lambda _: found[next(numbers)], shard)


def folded_in_pairs(pieces, combine):
    while len(jax.tree.leaves(pieces)[0]) > 1:
        pieces = jax.vmap(combine)(
            *(jax.tree.map(lambda part: part[side::2], pieces) for side in (0, 1))
        )
    return jax.tree.map(lambda part: part[0], pieces)


def carried_in(shard, axis, combine, identity):
    length, index = (lax.axis_size(axis), lax.axis_index(axis))
    passed = jnp.arange(length) < index

    def kept(part, zero, own):
        part = jnp.where(
            passed.reshape(-1, *(1 for _ in own.shape)), part, jnp.asarray(zero, own.dtype)
        )
        return part

    pieces = all_in_one(shard, axis)
    return folded_in_pairs(jax.tree.map(kept, pieces, identity, shard), combine)


def in_one_piece(arrays, axis, dim, along):
    both = jnp.concatenate(arrays, axis=along)
    result, at, outs = (lax.all_gather(both, axis, axis=dim, tiled=True), 0, [])
    for a in arrays:
        outs.append(lax.slice_in_dim(result, at, at + a.shape[along], axis=along))
        at += a.shape[along]
    return tuple(outs)


def chain(earlier, later):
    return (earlier[0] * later[0], later[0] * earlier[1] + later[1])


def body(
    tokens,
    norm_gain,
    w_recur_in,
    conv_weight,
    w_gate_decay,
    w_gate_input,
    decay_base,
    extra_decay,
    w_query,
    w_key,
    w_value,
    mix_lambda,
    head_gain,
    w_out_recur,
    w_out_attend,
    out_gain,
):
    row_count = tokens.shape[0]
    recur_cols = w_recur_in.shape[1]
    query_cols = w_query.shape[1]
    key_cols = w_key.shape[1]
    all_weights = jnp.concatenate([w_recur_in, w_query, w_key, w_value], axis=1)
    wide_piece = lax.all_gather(tokens, "tp", axis=1, tiled=True).astype(jnp.float32)
    scaled = (wide_piece * norm_gain).astype(jnp.bfloat16)
    accum = jnp.dot(scaled, all_weights, preferred_element_type=jnp.float32)
    squares = jnp.sum(wide_piece * wide_piece, axis=1, keepdims=True)
    accum, squares = (accum, squares)
    inverse = lax.rsqrt(squares / D + norm_eps)
    projected = (accum * inverse).astype(jnp.bfloat16)
    recur_in = projected[:, :recur_cols]
    queries = projected[:, recur_cols : recur_cols + query_cols]
    keys = projected[:, recur_cols + query_cols : recur_cols + query_cols + key_cols]
    values = projected[:, recur_cols + query_cols + key_cols :]
    taps = conv_weight.shape[0]
    carried_rows = shifted(recur_in[row_count - (taps - 1) :], "sp", 1)
    padded = jnp.concatenate([carried_rows, recur_in], axis=0).astype(jnp.float32)
    conv_acc = jnp.zeros((row_count, recur_cols), jnp.float32)
    for offset in range(taps):
        conv_acc = conv_acc + conv_weight[offset] * padded[offset : offset + row_count]
    conv_in = conv_acc.astype(jnp.bfloat16)
    gate_blocks = w_gate_decay.shape[0]
    blocks = conv_in.reshape(row_count, gate_blocks, HEAD)
    decay_gate = jax.nn.sigmoid(
        jnp.einsum("thi,hij->thj", blocks, w_gate_decay, preferred_element_type=jnp.float32)
    ).reshape(row_count, recur_cols)
    input_gate = jax.nn.sigmoid(
        jnp.einsum("thi,hij->thj", blocks, w_gate_input, preferred_element_type=jnp.float32)
    ).reshape(row_count, recur_cols)
    log_decay = -lru_rate * decay_gate * decay_base - jnp.repeat(extra_decay, HEAD, axis=1)
    decay = jnp.exp(log_decay)
    inject = jnp.sqrt(-jnp.expm1(2.0 * log_decay)) * input_gate * conv_in.astype(jnp.float32)
    decay_cum, local_state = lax.associative_scan(chain, (decay, inject), axis=0)
    identity = (jnp.ones((recur_cols,), jnp.float32), jnp.zeros((recur_cols,), jnp.float32))
    carried = carried_in(
        (decay_cum[row_count - 1], local_state[row_count - 1]), "sp", chain, identity
    )
    recur_out = (local_state + decay_cum * carried[1]).astype(jnp.bfloat16)
    kv_local = key_cols // (2 * HEAD)
    heads_local = query_cols // (2 * HEAD)
    group_size = heads_local // kv_local
    local_query = queries.reshape(row_count, kv_local, group_size, 2, HEAD)
    offset_rows = lax.axis_index("sp") * row_count
    positions = offset_rows + jnp.arange(row_count, dtype=jnp.int32)
    last_position = offset_rows + row_count - 1
    lambdas = mix_lambda.reshape(kv_local, group_size)
    start_state = (
        jnp.full((2, kv_local, group_size, row_count), -1e30, jnp.float32),
        jnp.zeros((2, kv_local, group_size, row_count), jnp.float32),
        jnp.zeros((2, row_count, kv_local, group_size, DV), jnp.float32),
    )
    key_piece, value_piece = in_one_piece((keys, values), "sp", 0, 1)
    count = key_piece.shape[0]

    def update(state):
        peaks, totals, attends = state
        key_three = key_piece.reshape(count, kv_local, 2, HEAD)
        value_three = value_piece.reshape(count, kv_local, DV)
        allowed = positions[:, None] >= jnp.arange(count, dtype=jnp.int32)[None, :]
        new_peaks, new_totals, new_attends = ([], [], [])
        for mapping in range(2):
            scores = jnp.einsum(
                "bkgd,tkd->kgbt",
                local_query[:, :, :, mapping, :],
                key_three[:, :, mapping, :],
                preferred_element_type=jnp.float32,
            ) * HEAD ** (-0.5)
            scores = jnp.where(allowed, scores, -jnp.inf)
            peak = jnp.maximum(peaks[mapping], jnp.max(scores, axis=-1))
            correction = jnp.exp(peaks[mapping] - peak)
            expo = jnp.exp(scores - peak[..., None])
            new_totals.append(totals[mapping] * correction + jnp.sum(expo, axis=-1))
            gained = jnp.einsum(
                "kgbt,tke->bkge",
                expo.astype(jnp.bfloat16),
                value_three,
                preferred_element_type=jnp.float32,
            )
            new_attends.append(
                attends[mapping] * jnp.transpose(correction, (2, 0, 1))[..., None] + gained
            )
            new_peaks.append(peak)
        return (jnp.stack(new_peaks), jnp.stack(new_totals), jnp.stack(new_attends))

    peaks, totals, attends = lax.cond(
        jnp.int32(0) <= last_position, update, lambda state: state, start_state
    )
    first = attends[0] / jnp.transpose(totals[0], (2, 0, 1))[..., None]
    second = attends[1] / jnp.transpose(totals[1], (2, 0, 1))[..., None]
    head_out = (first - lambdas[None, :, :, None] * second).reshape(row_count, heads_local, DV)
    normed = (
        head_out
        * lax.rsqrt(jnp.mean(head_out * head_out, axis=-1, keepdims=True) + norm_eps)
        * head_gain
    )
    attend_out = normed.astype(jnp.bfloat16).reshape(row_count, heads_local * DV)
    recur_rows, attend_rows = (
        lax.all_to_all(recur_out, "tp", split_axis=0, concat_axis=1, tiled=True),
        lax.all_to_all(attend_out, "tp", split_axis=0, concat_axis=1, tiled=True),
    )
    whole_recur, whole_attend = in_one_piece((w_out_recur, w_out_attend), "tp", 0, 1)
    merged = jnp.dot(recur_rows, whole_recur, preferred_element_type=jnp.float32) + jnp.dot(
        attend_rows, whole_attend, preferred_element_type=jnp.float32
    )
    final = (
        merged * lax.rsqrt(jnp.mean(merged * merged, axis=1, keepdims=True) + norm_eps) * out_gain
    )
    return final.astype(jnp.bfloat16)


def solution(mesh):
    in_specs = (
        P(("fs", "sp"), "tp"),
        P(),
        P(None, "tp"),
        P(None, "tp"),
        P("tp", None, None),
        P("tp", None, None),
        P("tp"),
        P(("fs", "sp"), "tp"),
        P(None, "tp"),
        P(None, "tp"),
        P(None, "tp"),
        P("tp"),
        P(),
        P("tp", None),
        P("tp", None),
        P(),
    )
    out_specs = P(("fs", "sp", "tp"), None)
    return jax.shard_map(body, mesh=mesh, in_specs=in_specs, out_specs=out_specs, check_vma=False)
```

profile of v0, /device:TPU:1, one launch (start us, length us, event | category | flops | bytes accessed | tf_op | source)
XLA Modules:
  0.0 134.3 jit_solution(11392075129574978183)
XLA Ops:
  6.5 5.3 %all_gather.9 = bf16[128,2048]{1,0:T(8,128)(2,1)S(1)} all-gather(bf16[128,1024]{1,0:T(8,128)(2,1)} %param.18), channel_id=1, replica_groups=mesh['sp'=32,'fs'=4,'tp'=2] {'tp'}, dimensions={1}, use_global_device_ids=true | all-gather | bytes 786432 | tf_op jit(solution)/shard_map/all_gather | solution.py:101
  12.1 3.3 %fusion.51 = bf16[128,1280]{1,0:T(8,128)(2,1)S(1)} fusion(bf16[2048,128]{1,0:T(8,128)(2,1)} %param.28, bf16[2048,128]{1,0:T(8,128)(2,1)} %param.27, bf16[2048,512]{1,0:T(8,128)(2,1)} %param.26, bf16[2048,512]{1,0:T(8,128)(2,1)} %param.20, bf16[128,2048]{1,0:T(8,128)(2,1)S(1)} %all_gather.9, f32[2048]{0:T(1024)} %param.19, f32[128]{0:T(128)S(1)} %add_rsqrt_fusion.2), kind=kOutput, calls=%fused_computation.54 | convolution fusion | flops 693174272 | bytes 6103552 | tf_op jit(solution)/shard_map/dot_general | solution.py:103
  15.4 0.6 concatenate.68
  16.2 1.6 %collective-permute-start = (bf16[3,512]{1,0:T(4,128)(2,1)S(1)}, bf16[3,512]{1,0:T(4,128)(2,1)S(1)}, u32[]{:S(2)}, u32[]{:S(2)}) collective-permute-start(bf16[3,512]{1,0:T(4,128)(2,1)S(1)} %slice.456), channel_id=1, source_target_pairs={{0,8},{8,16},{16,24},{24,32},{32,40},{40,48},{48,56},{56,64},{64,7... | collective-permute-start | bytes 9224 | tf_op jit(solution)/shard_map/ppermute | solution.py:18
  17.8 4.0 %pad_maximum_fusion.2 = bf16[512,4096]{1,0:T(8,128)(2,1)} fusion(bf16[512,2048]{1,0:T(8,128)(2,1)S(1)} %copy-done.2, bf16[512,2048]{1,0:T(8,128)(2,1)} %param.31), kind=kLoop, calls=%fused_computation.52 | loop fusion | flops 8388608 | bytes 8388608 | tf_op jit(solution)/shard_map/concatenate | solution.py:66
  22.4 0.3 fusion.59
  22.8 0.3 fusion.62
  23.2 0.3 convert_multiply_fusion.2
  26.5 0.7 broadcast_in_dim.59
  27.2 10.9 %all-to-all-start = ((f32[32,2,512]{2,1,0:T(2,128)}), f32[32,2,512]{2,1,0:T(2,128)S(1)}, u32[]{:S(2)}, u32[]{:S(2)}) async-start(f32[32,2,512]{2,1,0:T(2,128)} %broadcast_in_dim.59), calls=%async_computation | async-start | bytes 262144 | tf_op jit(solution)/shard_map/all_to_all | solution.py:23
  38.3 9.3 %all-to-all-done = f32[32,2,512]{2,1,0:T(2,128)S(1)} async-done(((f32[32,2,512]{2,1,0:T(2,128)}), f32[32,2,512]{2,1,0:T(2,128)S(1)}, u32[]{:S(2)}, u32[]{:S(2)}) %all-to-all-start) | async-done | bytes 131104 | tf_op jit(solution)/shard_map/all_to_all | solution.py:23
  48.3 5.4 %all_to_all.40 = bf16[2,64,512]{2,1,0:T(8,128)(2,1)S(1)} all-to-all(bf16[2,64,512]{2,1,0:T(8,128)(2,1)S(1)} %bitcast.173), channel_id=1, replica_groups=mesh['sp'=32,'fs'=4,'tp'=2] {'tp'}, dimensions={0} | all-to-all | bytes 262144 | tf_op jit(solution)/shard_map/all_to_all | solution.py:195
  53.7 37.1 %all-gather.5.cloned.1.call-done = bf16[4096,256]{1,0:T(8,128)(2,1)} async-done(((bf16[128,256]{1,0:T(8,128)(2,1)}), bf16[4096,256]{1,0:T(8,128)(2,1)}) %all-gather.5.cloned.1.call-update) | async-done | bytes 2097168 | tf_op jit(solution)/shard_map/all_gather | solution.py:67
  90.8 10.7 %conditional.1 = (f32[2,1,4,128]{3,2,1,0:T(4,128)S(1)}, f32[2,128,1,4,128]{4,1,3,2,0:T(8,128)S(1)}) conditional(s32[]{:T(128)} %convert_element_type.45, () %tuple.13, (s32[]{:T(128)}, s32[128]{0:T(128)S(1)}, bf16[4096,256]{1,0:T(8,128)(2,1)}, bf16[128,1280]{1,0:T(8,128)(2,1)S(1)}) %tuple.14), branch_computations={%region_1.2_spmd, %region_2.7_spmd} | conditional | flops 1640763520 | bytes 70309424 | solution.py:182
  90.8 0.2 copy.58
  91.1 1.3 slice.238
  92.4 0.5 copy.45
  92.9 0.3 iota_compare_fusion
  93.3 1.3 fusion.88
  94.6 1.1 fusion.1
  95.7 1.3 fusion.87
  97.0 1.1 fusion.3
  98.2 1.6 %fusion.21 = f32[1,128,1,4,128]{4,1,3,2,0:T(8,128)S(1)} fusion(f32[1,4,128,4096]{2,3,1,0:T(8,128)S(1)} %get-tuple-element.41, f32[4,128]{1,0:T(4,128)S(1)} %broadcast_maximum_fusion, bf16[4096,256]{1,0:T(8,128)(2,1)S(1)} %copy-done.1, f32[128,4]{0,1:T(4,128)S(1)} %get-tuple-element.45), kind=kOutput, calls=%fused_computation.18 | convolution fusion | flops 541130752 | bytes 9703424 | tf_op jit(solution)/shard_map/cond/branch_1_fun/kgbt,tke->bkge/dot_general | solution.py:170
  99.8 1.6 %fusion.27 = f32[1,128,1,4,128]{4,1,3,2,0:T(8,128)S(1)} fusion(f32[1,4,128,4096]{2,3,1,0:T(8,128)S(1)} %get-tuple-element.43, f32[4,128]{1,0:T(4,128)S(1)} %broadcast_maximum_fusion.1, bf16[4096,256]{1,0:T(8,128)(2,1)S(1)} %copy-done.1, f32[128,4]{0,1:T(4,128)S(1)} %get-tuple-element.36), kind=kOutput, calls=%fused_computation.20 | convolution fusion | flops 541130752 | bytes 9703424 | tf_op jit(solution)/shard_map/cond/branch_1_fun/kgbt,tke->bkge/dot_general | solution.py:170
  101.7 0.3 fusion.74
  102.2 0.2 mul.371
  102.9 0.2 div.79.clone
  103.9 9.0 %all_to_all.41 = bf16[2,64,512]{2,1,0:T(8,128)(2,1)S(1)} all-to-all(bf16[2,64,512]{2,1,0:T(8,128)(2,1)S(1)} %multiply_convert_fusion.1), channel_id=1, replica_groups=mesh['sp'=32,'fs'=4,'tp'=2] {'tp'}, dimensions={0} | all-to-all | bytes 262144 | tf_op jit(solution)/shard_map/all_to_all | solution.py:196
  112.9 7.5 %all-gather.3.cloned.1.call-done = bf16[1024,4096]{1,0:T(8,128)(2,1)} async-done(((bf16[512,4096]{1,0:T(8,128)(2,1)}), bf16[1024,4096]{1,0:T(8,128)(2,1)}) %all-gather.3.cloned.1.call-update) | async-done | bytes 8388624 | tf_op jit(solution)/shard_map/all_gather | solution.py:67
  120.4 3.0 %fusion.44 = f32[64,2048]{1,0:T(8,128)S(1)} fusion(bf16[64,1024]{1,0:T(8,128)(2,1)S(1)} %bitcast.180, bf16[1024,4096]{1,0:T(8,128)(2,1)} %all-gather.3.cloned.1.call-done), kind=kOutput, calls=%fused_computation.48 | convolution fusion | flops 268435456 | bytes 4849664 | tf_op jit(solution)/shard_map/dot_general | solution.py:199
  123.4 3.2 %multiply_reduce_fusion = (f32[64]{0:T(128)S(1)}, f32[64,2048]{1,0:T(8,128)S(1)}) fusion(f32[64,2048]{1,0:T(8,128)S(1)} %fusion.44, bf16[64,1024]{1,0:T(8,128)(2,1)S(1)} %bitcast.172, bf16[1024,4096]{1,0:T(8,128)(2,1)} %all-gather.3.cloned.1.call-done), kind=kOutput, calls=%fused_computation.69 | convolution fusion | flops 268828608 | bytes 5374208 | tf_op jit(solution)/shard_map/dot_general | solution.py:199
  126.6 0.8 multiply_convert_fusion
  (196 shorter events, 5.9 us)
Async XLA Ops:
  6.5 15.8 %copy-start = (bf16[8,64,64]{2,1,0:T(8,128)(2,1)S(1)}, bf16[8,64,64]{2,1,0:T(8,128)(2,1)}, u32[]{:S(2)}) copy-start(bf16[8,64,64]{2,1,0:T(8,128)(2,1)} %param.23) | copy-start | bytes 196612
  6.5 84.3 %all-gather.5.cloned.1.call-start = ((), (), s32[]{:S(2)}) async-start(), calls=%async_computation.4 | async-start | bytes 2162688 | tf_op jit(solution)/shard_map/all_gather | solution.py:67
  12.1 5.7 %copy-start.2 = (bf16[512,2048]{1,0:T(8,128)(2,1)S(1)}, bf16[512,2048]{1,0:T(8,128)(2,1)}, u32[]{:S(2)}) copy-start(bf16[512,2048]{1,0:T(8,128)(2,1)} %param.32) | copy-start | bytes 6291460
  15.4 6.4 %copy-start.4 = (f32[4,512]{1,0:T(4,128)S(1)}, f32[4,512]{1,0:T(4,128)}, u32[]{:S(2)}) copy-start(f32[4,512]{1,0:T(4,128)} %param.21) | copy-start | bytes 24580
  15.4 6.4 %copy-start.7 = (f32[512]{0:T(512)S(1)}, f32[512]{0:T(512)}, u32[]{:S(2)}) copy-start(f32[512]{0:T(512)} %param.24) | copy-start | bytes 6148
  15.4 6.4 %copy-start.5 = (f32[128,8]{0,1:T(8,128)S(1)}, f32[128,8]{0,1:T(8,128)}, u32[]{:S(2)}) copy-start(f32[128,8]{0,1:T(8,128)} %param.25) | copy-start | bytes 12292
  16.1 104.3 %all-gather.3.cloned.1.call-start = ((), (), s32[]{:S(2)}) async-start(), calls=%async_computation.3 | async-start | bytes 12582912 | tf_op jit(solution)/shard_map/all_gather | solution.py:67
  16.2 6.6 %copy-start.9 = (bf16[8,64,64]{2,1,0:T(8,128)(2,1)S(1)}, bf16[8,64,64]{2,1,0:T(8,128)(2,1)}, u32[]{:S(2)}) copy-start(bf16[8,64,64]{2,1,0:T(8,128)(2,1)} %param.22) | copy-start | bytes 196612
  16.2 5.9 %collective-permute-start = (bf16[3,512]{1,0:T(4,128)(2,1)S(1)}, bf16[3,512]{1,0:T(4,128)(2,1)S(1)}, u32[]{:S(2)}, u32[]{:S(2)}) collective-permute-start(bf16[3,512]{1,0:T(4,128)(2,1)S(1)} %slice.456), channel_id=1, source_target_pairs={{0,8},{8,16},{16,24},{24,32},{32,40},{40,48},{48,56},{56,64},{64,7... | collective-permute-start | bytes 9224 | tf_op jit(solution)/shard_map/ppermute | solution.py:18
  22.8 15.4 %copy-start.6 = (f32[4]{0:T(128)S(1)}, f32[4]{0:T(128)}, u32[]{:S(2)}) copy-start(f32[4]{0:T(128)} %param.29) | copy-start | bytes 52
  22.8 15.4 %copy-start.8 = (f32[128]{0:T(128)S(1)}, f32[128]{0:T(128)}, u32[]{:S(2)}) copy-start(f32[128]{0:T(128)} %param.30) | copy-start | bytes 1540
  27.2 20.4 %all-to-all-start = ((f32[32,2,512]{2,1,0:T(2,128)}), f32[32,2,512]{2,1,0:T(2,128)S(1)}, u32[]{:S(2)}, u32[]{:S(2)}) async-start(f32[32,2,512]{2,1,0:T(2,128)} %broadcast_in_dim.59), calls=%async_computation | async-start | bytes 262144 | tf_op jit(solution)/shard_map/all_to_all | solution.py:23
  95.7 2.5 %copy-start.1 = (bf16[4096,256]{1,0:T(8,128)(2,1)S(1)}, bf16[4096,256]{1,0:T(8,128)(2,1)}, u32[]{:S(2)}) copy-start(bf16[4096,256]{1,0:T(8,128)(2,1)} %get-tuple-element.22) | copy-start | bytes 6291460 | tf_op jit(solution)/shard_map/cond
  102.5 24.1 %copy-start.3 = (f32[2048]{0:T(1024)S(1)}, f32[2048]{0:T(1024)}, u32[]{:S(2)}) copy-start(f32[2048]{0:T(1024)} %param.33) | copy-start | bytes 24580
Sparse Core Ops, SparseCore 0:
  16.2 74.5 all-gather.4
  92.6 27.7 all-gather.2
where the time goes:
time: 135 us; the launch traced here: 134 us
  waiting for transfers between devices  54 us (40%)
  blocking collectives  19.7 us (15%)
  matrix products  15.9 us (12%)
  between operations  14.4 us (11%)
  starting transfers between devices  12.6 us (9%)
  other arithmetic  9.36 us (7%)
  local copies, waits for them, and re-layouts  8.21 us (6%)
    all_gather x2, waiting for transfers between devices, in_one_piece(): result, at, outs = (lax.all_gather(both, axis, axis=dim, tiled=True), 0, [])  44.6 us
    all_to_all x1, starting transfers between devices, copy_for_each(): return lax.all_to_all(copies, axis, split_axis=0, concat_axis=0, tiled=True)  10.9 us
    all_to_all x1, waiting for transfers between devices, copy_for_each(): return lax.all_to_all(copies, axis, split_axis=0, concat_axis=0, tiled=True)  9.34 us
    all_to_all x1, blocking collectives, body(): lax.all_to_all(attend_out, 'tp', split_axis=0, concat_axis=1, tiled=True)  8.96 us
    all_to_all x1, blocking collectives, body(): lax.all_to_all(recur_out, 'tp', split_axis=0, concat_axis=1, tiled=True)  5.39 us
    all_gather x1, blocking collectives, body(): lax.all_gather(tokens, 'tp', axis=1, tiled=True).astype(jnp.float32)  5.34 us
    concatenate x1, other arithmetic, in_one_piece(): both = jnp.concatenate(arrays, axis=along)  3.96 us
    dot_general x1, matrix products, body(): accum = jnp.dot(scaled, all_weights, preferred_element_type=jnp.float32)  3.32 us
  transfers between devices with their start and end apart: 4, of which 3 were waited for; matrix products, arithmetic and copies ran while one was open for 17% of the time, Pallas kernels for 0%

commit v1 on v0

v1 whole, which is shorter than its diff:
```python
import jax
import jax.numpy as jnp
from jax import lax
from jax.experimental import pallas as pl
from jax.experimental.pallas import tpu as pltpu
from jax.sharding import PartitionSpec as P

MESH = pl.DeviceIdType.MESH
BF = jnp.bfloat16
F32 = jnp.float32

D = 2048
HALF = 1024
HEAD = 64
ROWS = 128
ZN = 8
YN = 4
SP = ZN * YN
RATE = 8.0
EPS = 1e-06
FWD = 4
BACK = 3
NSEND = 96


def dot(a, b):
    return jnp.dot(a, b, preferred_element_type=F32)


def minus_expm1(x):
    series = 1.0 + x * (
        1 / 2 + x * (1 / 6 + x * (1 / 24 + x * (1 / 120 + x * (1 / 720 + x * (1 / 5040 + x / 40320)))))
    )
    return jnp.where(x > -0.5, -x * series, 1.0 - jnp.exp(x))


def kernel(
    tok_h, gain_h, wr_h, cw_h, wgd_h, wgi_h, base_h, extra_h, wq_h, wk_h, wv_h, lam_h, hgain_h,
    wor_h, woa_h, ogain_h, out_h,
    tok, gain, wr, cw, wgd, wgi, base, extra, wq, wkv, lam, hgain, wor, woa, ogain,
    scaled, acc, kbuf, vbuf, rin, halo, xext, qt, att, peak, total, gates,
    crow, ctot, decs, states, mbuf, mrecv, outv,
    lsem, ssem, tsem, ksem, vsem, hsem, crsem, ctsem, msem,
):
    sp = lax.axis_index("sp")
    c = lax.axis_index("tp")
    z = sp // YN
    y = sp % YN

    locals_ = []

    def load(src, dst):
        copy = pltpu.make_async_copy(src, dst, lsem.at[len(locals_)])
        locals_.append(copy)
        copy.start()
        return copy

    own_rows = pl.ds(pl.multiple_of(c * HALF, HALF), HALF)
    other_rows = pl.ds(pl.multiple_of((1 - c) * HALF, HALF), HALF)
    l_tok = load(tok_h, tok.at[c])
    l_gain = load(gain_h, gain)
    l_own = [
        load(wk_h.at[own_rows], wkv.at[own_rows, pl.ds(0, 128)]),
        load(wv_h.at[own_rows], wkv.at[own_rows, pl.ds(128, 128)]),
        load(wr_h.at[own_rows], wr.at[own_rows]),
        load(wq_h.at[own_rows], wq.at[own_rows]),
    ]
    l_kv = [
        load(wk_h.at[other_rows], wkv.at[other_rows, pl.ds(0, 128)]),
        load(wv_h.at[other_rows], wkv.at[other_rows, pl.ds(128, 128)]),
    ]
    l_r = load(wr_h.at[other_rows], wr.at[other_rows])
    l_q = load(wq_h.at[other_rows], wq.at[other_rows])
    l_small = [
        load(cw_h, cw), load(wgd_h, wgd), load(wgi_h, wgi), load(base_h, base), load(extra_h, extra),
        load(lam_h, lam), load(hgain_h, hgain), load(ogain_h, ogain),
    ]

    barrier = pltpu.get_barrier_semaphore()
    pl.semaphore_signal(barrier, inc=1, device_id={"tp": 1 - c}, device_id_type=MESH)
    for step in (1, 2, 3):
        pl.semaphore_signal(
            barrier, inc=1, device_id={"sp": z * YN + (y + step) % YN}, device_id_type=MESH
        )
    for step in (1, ZN - 1):
        pl.semaphore_signal(
            barrier, inc=1, device_id={"sp": ((z + step) % ZN) * YN + y}, device_id_type=MESH
        )
    for step in (1, SP - 1):
        pl.semaphore_signal(
            barrier, inc=1, device_id={"sp": (sp + step) % SP}, device_id_type=MESH
        )

    sends = []

    def send(src, dst, rsem, when=None, **target):
        copy = pltpu.make_async_remote_copy(
            src_ref=src, dst_ref=dst, send_sem=ssem.at[len(sends)], recv_sem=rsem,
            device_id=target, device_id_type=MESH,
        )
        sends.append((copy, when))
        if when is None:
            copy.start()
        else:
            pl.when(when)(lambda: copy.start())

    def arrived(dst, rsem, when=None):
        copy = pltpu.make_async_remote_copy(
            src_ref=dst, dst_ref=dst, send_sem=ssem.at[0], recv_sem=rsem,
            device_id={"tp": 1 - c}, device_id_type=MESH,
        )
        if when is None:
            copy.wait_recv()
        else:
            pl.when(when)(lambda: copy.wait_recv())

    up = ((z + 1) % ZN) * YN + y
    down = ((z + ZN - 1) % ZN) * YN + y

    def beside(step):
        return z * YN + (y + step + YN) % YN

    l_tok.wait()
    pl.semaphore_wait(barrier, 8)
    send(tok.at[c], tok.at[c], tsem, tp=1 - c)
    l_wor = load(wor_h, wor)
    l_woa = load(woa_h, woa)

    l_gain.wait()

    def scale_half(half):
        x = tok[half].astype(F32)
        scaled[half] = (x * gain[half]).astype(BF)
        return jnp.sum(x * x, axis=1, keepdims=True)

    squares = scale_half(c)
    for copy in l_own:
        copy.wait()
    acc[:, 0:256] = dot(scaled[c], wkv[own_rows, :])
    acc[:, 256:768] = dot(scaled[c], wr[own_rows, :])
    acc[:, 768:1280] = dot(scaled[c], wq[own_rows, :])

    arrived(tok.at[1 - c], tsem)
    squares = squares + scale_half(1 - c)
    inverse = lax.rsqrt(squares / D + EPS)
    for copy in l_kv:
        copy.wait()
    kv = (acc[:, 0:256] + dot(scaled[1 - c], wkv[other_rows, :])) * inverse
    kbuf[sp] = kv[:, 0:128].astype(BF)
    vbuf[sp] = jnp.transpose(kv[:, 128:256]).astype(BF)

    def slot(row, col):
        return row * YN + col

    def send_block(buf, sem, row, col, to, when):
        s = slot(row, col)
        send(buf.at[s], buf.at[s], sem.at[s], when=when, sp=to)

    has_up = z < ZN - 1
    goes_down = z <= BACK - 1

    def forward_own(buf, sem, col):
        send_block(buf, sem, z, col, up, has_up)
        send_block(buf, sem, z, col, down, goes_down)

    forward_own(vbuf, vsem, y)
    for step in (1, 3, 2):
        send(kbuf.at[sp], kbuf.at[sp], ksem.at[sp], sp=beside(step))
    forward_own(kbuf, ksem, y)

    def plus(buf, sem, d, col):
        row = jnp.maximum(z - d, 0)
        ok = z >= d
        s = slot(row, col)
        arrived(buf.at[s], sem.at[s], ok)
        if d < FWD:
            send_block(buf, sem, row, col, up, ok & has_up)

    def minus(buf, sem, e, col):
        row = (z + e) % ZN
        ok = row <= BACK - 1
        s = slot(row, col)
        arrived(buf.at[s], sem.at[s], ok)
        if e < BACK:
            send_block(buf, sem, row, col, down, ok)

    def row_plus(d):
        return jnp.maximum(z - d, 0), z >= d

    def row_minus(e):
        row = (z + e) % ZN
        return row, (row <= BACK - 1) & (z > row)

    def spread_v(row, ok):
        way = 1 - 2 * (row % 2)
        send_block(vbuf, vsem, row, y, beside(way), ok)
        send_block(vbuf, vsem, row, y, beside(-way), ok)

    def relay_v(row, ok):
        way = 1 - 2 * (row % 2)
        s = slot(row, (y - way + YN) % YN)
        arrived(vbuf.at[s], vsem.at[s], ok)
        send(vbuf.at[s], vbuf.at[s], vsem.at[s], when=ok, sp=beside(way))

    def finish_v(row, ok):
        way = 1 - 2 * (row % 2)
        for col in ((y + way + YN) % YN, (y + 2) % YN):
            s = slot(row, col)
            arrived(vbuf.at[s], vsem.at[s], ok)

    always = z >= 0
    spread_v(z, always)

    l_r.wait()
    recur = ((acc[:, 256:768] + dot(scaled[1 - c], wr[other_rows, :])) * inverse).astype(BF)
    rin[...] = recur
    send(rin.at[pl.ds(ROWS - 16, 16)], halo, hsem, when=sp < SP - 1, sp=(sp + 1) % SP)
    xext[pl.ds(8, ROWS), :] = recur.astype(F32)

    l_q.wait()
    query = ((acc[:, 768:1280] + dot(scaled[1 - c], wq[other_rows, :])) * inverse).astype(BF)
    query = query.astype(F32) * HEAD ** (-0.5)
    qt[...] = jnp.zeros_like(qt)
    for h in range(4):
        turned = jnp.transpose(query[:, h * 128 : (h + 1) * 128]).astype(BF)
        lanes = slice((h % 2) * 128, (h % 2) * 128 + 128)
        qt[h // 2, 0:64, lanes] = turned[0:64]
        qt[2 + h // 2, 64:128, lanes] = turned[64:128]

    for step in (1, 3, 2):
        col = (y + step) % YN
        s = slot(z, col)
        arrived(kbuf.at[s], ksem.at[s])
        forward_own(kbuf, ksem, col)

    plus(vbuf, vsem, 1, y)
    minus(vbuf, vsem, 1, y)
    spread_v(*row_plus(1))
    spread_v(*row_minus(1))
    plus(kbuf, ksem, 1, y)
    minus(kbuf, ksem, 1, y)
    relay_v(z, always)

    for copy in l_small:
        copy.wait()
    arrived(halo, hsem, sp > 0)
    before = halo[8:16, :].astype(F32)
    xext[pl.ds(0, 8), :] = jnp.where(sp > 0, before, 0.0)
    conv = jnp.zeros((ROWS, 512), F32)
    for k in range(4):
        conv = conv + cw[k : k + 1, :] * xext[pl.ds(5 + k, ROWS), :]
    conv = conv.astype(BF)
    gates[...] = jnp.zeros_like(gates)
    for j in range(4):
        for side in range(2):
            rows = slice(side * 64, side * 64 + 64)
            gates[j, rows, side * 64 : side * 64 + 64] = wgd[2 * j + side]
            gates[j, rows, 128 + side * 64 : 128 + side * 64 + 64] = wgi[2 * j + side]
    lane = lax.broadcasted_iota(jnp.int32, (ROWS, 128), 1)
    line = lax.broadcasted_iota(jnp.int32, (ROWS, 128), 0)
    for j in range(4):
        cols = slice(j * 128, j * 128 + 128)
        part = conv[:, cols]
        both = dot(part, gates[j])
        decay_gate = jax.nn.sigmoid(both[:, 0:128])
        input_gate = jax.nn.sigmoid(both[:, 128:256])
        added = jnp.where(lane < 64, extra[:, 2 * j : 2 * j + 1], extra[:, 2 * j + 1 : 2 * j + 2])
        log_decay = -RATE * decay_gate * base[:, cols] - added
        a = jnp.exp(log_decay)
        b = jnp.sqrt(minus_expm1(2.0 * log_decay)) * input_gate * part.astype(F32)
        for shift in (1, 2, 4, 8, 16, 32, 64):
            inside = line >= shift
            a_back = jnp.where(inside, pltpu.roll(a, shift, 0), 1.0)
            b_back = jnp.where(inside, pltpu.roll(b, shift, 0), 0.0)
            b = a * b_back + b
            a = a * a_back
        decs[:, cols] = a
        states[:, cols] = b
        crow[y, 0:1, cols] = a[ROWS - 1 : ROWS]
        crow[y, 1:2, cols] = b[ROWS - 1 : ROWS]
    for step in (1, 3, 2):
        send(crow.at[y], crow.at[y], crsem.at[y], sp=beside(step))

    def plus_keys(d):
        for step in (1, 3, 2):
            plus(kbuf, ksem, d, (y + step) % YN)

    def minus_keys(e):
        for step in (1, 3, 2):
            minus(kbuf, ksem, e, (y + step) % YN)

    def attend(row, ok, diagonal):
        def all_chunks():
            first = row * YN
            keys = kbuf[pl.ds(first, YN)].reshape(YN * ROWS, 128)
            values = jnp.concatenate([vbuf[first + i] for i in range(YN)], axis=1)

            def one(chunk, carry):
                scores = dot(keys, qt[chunk])
                if diagonal:
                    key_at = lax.broadcasted_iota(jnp.int32, scores.shape, 0)
                    query_at = lax.broadcasted_iota(jnp.int32, scores.shape, 1) % ROWS + y * ROWS
                    scores = jnp.where(query_at >= key_at, scores, -1e30)
                old = peak[chunk]
                new = jnp.maximum(old, jnp.max(scores, axis=0, keepdims=True))
                weights = jnp.exp(scores - new)
                fade = jnp.exp(old - new)
                total[chunk] = total[chunk] * fade + jnp.sum(weights, axis=0, keepdims=True)
                att[chunk] = att[chunk] * fade + dot(values, weights.astype(BF))
                peak[chunk] = new
                return carry

            lax.fori_loop(0, 4, one, 0)

        if ok is None:
            all_chunks()
        else:
            pl.when(ok)(all_chunks)

    plus_keys(1)
    minus_keys(1)
    peak[...] = jnp.full_like(peak, -1e30)
    total[...] = jnp.zeros_like(total)
    att[...] = jnp.zeros_like(att)
    finish_v(z, always)
    attend(z, None, True)

    relay_v(*row_plus(1))
    relay_v(*row_minus(1))
    plus(vbuf, vsem, 2, y)
    minus(vbuf, vsem, 2, y)
    spread_v(*row_plus(2))
    spread_v(*row_minus(2))

    for step in (1, 3, 2):
        col = (y + step) % YN
        arrived(crow.at[col], crsem.at[col])
    all_a = crow[0, 0:1, :]
    all_s = crow[0, 1:2, :]
    for col in range(1, YN):
        all_s = crow[col, 0:1, :] * all_s + crow[col, 1:2, :]
        all_a = crow[col, 0:1, :] * all_a
    ctot[z, 0:1, :] = all_a
    ctot[z, 1:2, :] = all_s
    send(ctot.at[z], ctot.at[z], ctsem.at[z], when=has_up, sp=up)
    send(ctot.at[z], ctot.at[z], ctsem.at[z], when=goes_down, sp=down)

    def plus_carry(d):
        row, ok = row_plus(d)
        arrived(ctot.at[row], ctsem.at[row], ok)
        if d < FWD:
            send(ctot.at[row], ctot.at[row], ctsem.at[row], when=ok & has_up, sp=up)

    def minus_carry(e):
        row = (z + e) % ZN
        ok = row <= BACK - 1
        arrived(ctot.at[row], ctsem.at[row], ok)
        if e < BACK:
            send(ctot.at[row], ctot.at[row], ctsem.at[row], when=ok, sp=down)

    plus(kbuf, ksem, 2, y)
    minus(kbuf, ksem, 2, y)
    plus_keys(2)
    minus_keys(2)
    finish_v(*row_plus(1))
    finish_v(*row_minus(1))
    attend(*row_plus(1), False)
    plus_carry(1)
    minus_carry(1)
    relay_v(*row_plus(2))
    relay_v(*row_minus(2))
    plus(vbuf, vsem, 3, y)
    minus(vbuf, vsem, 3, y)
    spread_v(*row_plus(3))
    spread_v(*row_minus(3))
    plus(kbuf, ksem, 3, y)
    minus(kbuf, ksem, 3, y)
    attend(*row_minus(1), False)
    plus_carry(2)
    minus_carry(2)
    plus_keys(3)
    minus_keys(3)
    finish_v(*row_plus(2))
    finish_v(*row_minus(2))
    attend(*row_plus(2), False)
    plus_carry(3)
    minus_carry(3)
    relay_v(*row_plus(3))
    relay_v(*row_minus(3))
    plus(vbuf, vsem, 4, y)
    spread_v(*row_plus(4))
    plus(kbuf, ksem, 4, y)
    attend(*row_minus(2), False)
    plus_carry(4)

    def fold_total(row, s):
        return ctot[row, 0:1, :] * s + ctot[row, 1:2, :]

    def fold_row(col, s):
        return crow[col, 0:1, :] * s + crow[col, 1:2, :]

    carry_in = lax.fori_loop(0, z, fold_total, jnp.zeros((1, 512), F32))
    carry_in = lax.fori_loop(0, y, fold_row, carry_in)
    recur_out = (states[...] + decs[...] * carry_in).astype(BF)
    l_wor.wait()
    for n in range(4):
        mbuf[n] = dot(recur_out, wor[:, n * 512 : n * 512 + 512])

    finish_v(*row_plus(3))
    finish_v(*row_minus(3))
    attend(*row_plus(3), False)
    relay_v(*row_plus(4))
    attend(*row_minus(3), False)
    plus_keys(4)
    finish_v(*row_plus(4))
    attend(*row_plus(4), False)

    pieces = []
    for h in range(4):
        lanes = slice((h % 2) * 128, (h % 2) * 128 + 128)
        first = att[h // 2, :, lanes] / total[h // 2, :, lanes]
        second = att[2 + h // 2, :, lanes] / total[2 + h // 2, :, lanes]
        out = first - lam[0:1, h : h + 1] * second
        out = out * lax.rsqrt(jnp.mean(out * out, axis=0, keepdims=True) + EPS)
        pieces.append((jnp.transpose(out) * hgain[...]).astype(BF))
    attend_out = jnp.concatenate(pieces, axis=1)

    mine = pl.ds(pl.multiple_of(c * 64, 64), 64)
    theirs = pl.ds(pl.multiple_of((1 - c) * 64, 64), 64)
    l_woa.wait()
    for n in range(4):
        mbuf[n] += dot(attend_out, woa[:, n * 512 : n * 512 + 512])
        send(mbuf.at[n, theirs], mrecv.at[n], msem.at[n], tp=1 - c)
    power = jnp.zeros((64, 1), F32)
    for n in range(4):
        arrived(mrecv.at[n], msem.at[n])
        whole = mbuf[n, mine, :] + mrecv[n]
        mrecv[n] = whole
        power = power + jnp.sum(whole * whole, axis=1, keepdims=True)
    scale = lax.rsqrt(power / D + EPS)
    for n in range(4):
        cols = slice(n * 512, n * 512 + 512)
        outv[:, cols] = (mrecv[n] * scale * ogain[:, cols]).astype(BF)
    last = load(outv, out_h)
    for copy, when in sends:
        if when is None:
            copy.wait_send()
        else:
            pl.when(when)(lambda copy=copy: copy.wait_send())
    last.wait()


def body(
    tokens, norm_gain, w_recur_in, conv_weight, w_gate_decay, w_gate_input, decay_base, extra_decay,
    w_query, w_key, w_value, mix_lambda, head_gain, w_out_recur, w_out_attend, out_gain,
):
    any_ = pl.BlockSpec(memory_space=pl.ANY)
    vmem = pltpu.VMEM
    dma = pltpu.SemaphoreType.DMA
    scratch = [
        vmem((2, ROWS, HALF), BF), vmem((2, 1, HALF), F32), vmem((D, 512), BF), vmem((4, 512), F32),
        vmem((8, 64, 64), BF), vmem((8, 64, 64), BF), vmem((1, 512), F32), vmem((ROWS, 8), F32),
        vmem((D, 512), BF), vmem((D, 256), BF), vmem((1, 4), F32), vmem((1, 128), F32),
        vmem((512, D), BF), vmem((512, D), BF), vmem((1, D), F32),
        vmem((2, ROWS, HALF), BF), vmem((ROWS, 1280), F32),
        vmem((SP, ROWS, 128), BF), vmem((SP, 128, ROWS), BF),
        vmem((ROWS, 512), BF), vmem((16, 512), BF), vmem((ROWS + 8, 512), F32),
        vmem((4, 128, 256), BF), vmem((4, 128, 256), F32), vmem((4, 1, 256), F32), vmem((4, 1, 256), F32),
        vmem((4, 128, 256), BF),
        vmem((YN, 2, 512), F32), vmem((ZN, 2, 512), F32), vmem((ROWS, 512), F32), vmem((ROWS, 512), F32),
        vmem((4, ROWS, 512), F32), vmem((4, 64, 512), F32), vmem((64, D), BF),
        dma((24,)), dma((NSEND,)), dma, dma((SP,)), dma((SP,)), dma, dma((YN,)), dma((ZN,)), dma((4,)),
    ]
    return pl.pallas_call(
        kernel,
        out_shape=jax.ShapeDtypeStruct((64, D), BF),
        in_specs=[any_] * 16,
        out_specs=any_,
        scratch_shapes=scratch,
        compiler_params=pltpu.CompilerParams(
            collective_id=0, has_side_effects=True, vmem_limit_bytes=60 * 1024 * 1024
        ),
        name="layer",
    )(
        tokens, norm_gain.reshape(2, 1, HALF), w_recur_in, conv_weight, w_gate_decay, w_gate_input,
        decay_base.reshape(1, -1), extra_decay, w_query, w_key, w_value, mix_lambda.reshape(1, -1),
        head_gain.reshape(1, -1), w_out_recur, w_out_attend, out_gain.reshape(1, -1),
    )


def solution(mesh):
    in_specs = (
        P(("fs", "sp"), "tp"),
        P(),
        P(None, "tp"),
        P(None, "tp"),
        P("tp", None, None),
        P("tp", None, None),
        P("tp"),
        P(("fs", "sp"), "tp"),
        P(None, "tp"),
        P(None, "tp"),
        P(None, "tp"),
        P("tp"),
        P(),
        P("tp", None),
        P("tp", None),
        P(),
    )
    out_specs = P(("fs", "sp", "tp"), None)
    return jax.shard_map(body, mesh=mesh, in_specs=in_specs, out_specs=out_specs, check_vma=False)
```

time: 135 us -> 47.5 us (0.35)
  the two profiles are of different devices: /device:TPU:1 before, /device:TPU:193 now
where the time goes in v1:
time: 47.5 us; the launch traced here: 47.4 us
  Pallas kernels  44.3 us (93%)
  local copies, waits for them, and re-layouts  3.08 us (6%)
    pallas_call x1, Pallas kernels, body(): pl.pallas_call(kernel, out_shape=jax.ShapeDtypeStruct((64, D), BF), in_sp...  44.3 us
    unnamed x2, local copies, waits for them, and re-layouts  3.08 us

profile of v1, /device:TPU:193, one launch (start us, length us, event | category | flops | bytes accessed | tf_op | source)
XLA Modules:
  0.0 47.4 jit_solution(2872404047142424226)
XLA Ops:
  0.0 1.4 %copy.17.extra_h = f32[128,8]{1,0:T(8,128)} copy(f32[128,8]{0,1:T(8,128)} %param.23) | data formatting | bytes 8192 | tf_op args[7]
  1.4 44.3 %layer.1 = bf16[64,2048]{1,0:T(8,128)(2,1)} custom-call(bf16[128,1024]{1,0:T(8,128)(2,1)} %tok_h.1, f32[2,1,1024]{2,1,0:T(1,128)} %bitcast.5, bf16[2048,512]{1,0:T(8,128)(2,1)} %wr_h.1, f32[4,512]{1,0:T(4,128)} %cw_h.1, bf16[8,64,64]{2,1,0:T(8,128)(2,1)} %wgd_h.1, bf16[8,64,64]{2,1,0:T(8,128)(2,1)} %wgi_h.1, f32[1,512]{1,0:T(1,128)} %bitcast.7, ...), custom_call_target="tpu_custom_call" | custom-call | tf_op jit(solution)/shard_map/layer/pallas_call | solution.py:474
  45.7 1.7 %copy.19 = bf16[64,2048]{1,0:T(8,128)(2,1)} copy(bf16[64,2048]{1,0:T(8,128)(2,1)} %layer.1) | data formatting | bytes 524288

commit v2 on v1

--- a/solution.py
+++ b/solution.py
@@ -20,7 +20,7 @@
 EPS = 1e-06
 FWD = 4
 BACK = 3
-NSEND = 96
+NSEND = 144
 
 
 def dot(a, b):
@@ -39,8 +39,8 @@
     wor_h, woa_h, ogain_h, out_h,
     tok, gain, wr, cw, wgd, wgi, base, extra, wq, wkv, lam, hgain, wor, woa, ogain,
     scaled, acc, kbuf, vbuf, rin, halo, xext, qt, att, peak, total, gates,
-    crow, ctot, decs, states, mbuf, mrecv, outv,
-    lsem, ssem, tsem, ksem, vsem, hsem, crsem, ctsem, msem,
+    crow, ctot, decs, states, mbuf, mrecv, rout,
+    lsem, ssem, tsem, ksem, vsem, hsem, crsem, ctsem, msem, insem,
 ):
     sp = lax.axis_index("sp")
     c = lax.axis_index("tp")
@@ -82,14 +82,21 @@
         pl.semaphore_signal(
             barrier, inc=1, device_id={"sp": z * YN + (y + step) % YN}, device_id_type=MESH
         )
-    for step in (1, ZN - 1):
-        pl.semaphore_signal(
-            barrier, inc=1, device_id={"sp": ((z + step) % ZN) * YN + y}, device_id_type=MESH
-        )
-    for step in (1, SP - 1):
-        pl.semaphore_signal(
-            barrier, inc=1, device_id={"sp": (sp + step) % SP}, device_id_type=MESH
-        )
+    has_up = z < ZN - 1
+    has_down = z > 0
+    corner_up = (y == YN - 1) & has_up
+    corner_down = (y == 0) & has_down
+    greeted = 4
+    for when, target in (
+        (has_up, (z + 1) * YN + y), (has_down, (z - 1) * YN + y), (corner_up, sp + 1), (corner_down, sp - 1)
+    ):
+        near = jnp.where(when, target, sp)
+
+        @pl.when(when)
+        def _():
+            pl.semaphore_signal(barrier, inc=1, device_id={"sp": near}, device_id_type=MESH)
+
+        greeted = greeted + when.astype(jnp.int32)
 
     sends = []
 
@@ -117,12 +124,21 @@
     up = ((z + 1) % ZN) * YN + y
     down = ((z + ZN - 1) % ZN) * YN + y
 
+    def pass_in(k):
+        @pl.when(z == ZN - 1 - k)
+        def _():
+            if k > 0:
+                pl.semaphore_wait(insem, 1)
+            if k < ZN - 1:
+                pl.semaphore_signal(insem, inc=1, device_id={"sp": down}, device_id_type=MESH)
+
     def beside(step):
         return z * YN + (y + step + YN) % YN
 
     l_tok.wait()
-    pl.semaphore_wait(barrier, 8)
+    pl.semaphore_wait(barrier, greeted)
     send(tok.at[c], tok.at[c], tsem, tp=1 - c)
+    pass_in(0)
     l_wor = load(wor_h, wor)
     l_woa = load(woa_h, woa)
 
@@ -156,12 +172,20 @@
         s = slot(row, col)
         send(buf.at[s], buf.at[s], sem.at[s], when=when, sp=to)
 
-    has_up = z < ZN - 1
     goes_down = z <= BACK - 1
+    postponed = []
+
+    def send_down(buf, sem, at, when):
+        send(buf.at[at], buf.at[at], sem.at[at], when=when & has_down, sp=down)
+        wrap = lambda: send(buf.at[at], buf.at[at], sem.at[at], when=when & (z == 0), sp=down)
+        if postponed is None:
+            wrap()
+        else:
+            postponed.append(wrap)
 
     def forward_own(buf, sem, col):
         send_block(buf, sem, z, col, up, has_up)
-        send_block(buf, sem, z, col, down, goes_down)
+        send_down(buf, sem, slot(z, col), goes_down)
 
     forward_own(vbuf, vsem, y)
     for step in (1, 3, 2):
@@ -182,7 +206,7 @@
         s = slot(row, col)
         arrived(buf.at[s], sem.at[s], ok)
         if e < BACK:
-            send_block(buf, sem, row, col, down, ok)
+            send_down(buf, sem, s, ok)
 
     def row_plus(d):
         return jnp.maximum(z - d, 0), z >= d
@@ -216,6 +240,16 @@
     rin[...] = recur
     send(rin.at[pl.ds(ROWS - 16, 16)], halo, hsem, when=sp < SP - 1, sp=(sp + 1) % SP)
     xext[pl.ds(8, ROWS), :] = recur.astype(F32)
+
+    pass_in(1)
+
+    def v_plus(d):
+        plus(vbuf, vsem, d, y)
+        spread_v(*row_plus(d))
+
+    def v_minus(e):
+        minus(vbuf, vsem, e, y)
+        spread_v(*row_minus(e))
 
     l_q.wait()
     query = ((acc[:, 768:1280] + dot(scaled[1 - c], wq[other_rows, :])) * inverse).astype(BF)
@@ -227,18 +261,16 @@
         qt[h // 2, 0:64, lanes] = turned[0:64]
         qt[2 + h // 2, 64:128, lanes] = turned[64:128]
 
+    pass_in(2)
+    v_plus(1)
+
     for step in (1, 3, 2):
         col = (y + step) % YN
         s = slot(z, col)
         arrived(kbuf.at[s], ksem.at[s])
         forward_own(kbuf, ksem, col)
-
-    plus(vbuf, vsem, 1, y)
-    minus(vbuf, vsem, 1, y)
-    spread_v(*row_plus(1))
-    spread_v(*row_minus(1))
     plus(kbuf, ksem, 1, y)
-    minus(kbuf, ksem, 1, y)
+    pass_in(3)
     relay_v(z, always)
 
     for copy in l_small:
@@ -258,13 +290,14 @@
             gates[j, rows, 128 + side * 64 : 128 + side * 64 + 64] = wgi[2 * j + side]
     lane = lax.broadcasted_iota(jnp.int32, (ROWS, 128), 1)
     line = lax.broadcasted_iota(jnp.int32, (ROWS, 128), 0)
-    for j in range(4):
+    extra_t = jnp.transpose(extra[...])
+    def recur_columns(j):
         cols = slice(j * 128, j * 128 + 128)
         part = conv[:, cols]
         both = dot(part, gates[j])
         decay_gate = jax.nn.sigmoid(both[:, 0:128])
         input_gate = jax.nn.sigmoid(both[:, 128:256])
-        added = jnp.where(lane < 64, extra[:, 2 * j : 2 * j + 1], extra[:, 2 * j + 1 : 2 * j + 2])
+        added = jnp.where(lane < 64, extra_t[:, 2 * j : 2 * j + 1], extra_t[:, 2 * j + 1 : 2 * j + 2])
         log_decay = -RATE * decay_gate * base[:, cols] - added
         a = jnp.exp(log_decay)
         b = jnp.sqrt(minus_expm1(2.0 * log_decay)) * input_gate * part.astype(F32)
@@ -278,120 +311,102 @@
         states[:, cols] = b
         crow[y, 0:1, cols] = a[ROWS - 1 : ROWS]
         crow[y, 1:2, cols] = b[ROWS - 1 : ROWS]
+
+    pass_in(4)
+    recur_columns(0)
+    v_plus(2)
+    v_minus(1)
+    pass_in(5)
+    recur_columns(1)
+    recur_columns(2)
+    v_minus(2)
+    pass_in(6)
+    recur_columns(3)
     for step in (1, 3, 2):
         send(crow.at[y], crow.at[y], crsem.at[y], sp=beside(step))
-
-    def plus_keys(d):
-        for step in (1, 3, 2):
-            plus(kbuf, ksem, d, (y + step) % YN)
-
-    def minus_keys(e):
-        for step in (1, 3, 2):
-            minus(kbuf, ksem, e, (y + step) % YN)
-
-    def attend(row, ok, diagonal):
-        def all_chunks():
-            first = row * YN
-            keys = kbuf[pl.ds(first, YN)].reshape(YN * ROWS, 128)
-            values = jnp.concatenate([vbuf[first + i] for i in range(YN)], axis=1)
-
-            def one(chunk, carry):
-                scores = dot(keys, qt[chunk])
-                if diagonal:
-                    key_at = lax.broadcasted_iota(jnp.int32, scores.shape, 0)
-                    query_at = lax.broadcasted_iota(jnp.int32, scores.shape, 1) % ROWS + y * ROWS
-                    scores = jnp.where(query_at >= key_at, scores, -1e30)
-                old = peak[chunk]
+    pass_in(7)
+    for wrap in postponed:
+        wrap()
+    postponed = None
+    relay_v(*row_plus(1))
+
+    def key(sign, n, step):
+        move = plus if sign > 0 else minus
+        return lambda: move(kbuf, ksem, n, (y + step) % YN)
+
+    def attend(row, ok, part, diagonal=False, steps=None):
+        def run():
+            if steps is None:
+                first = row * YN
+                keys = kbuf[pl.ds(first, YN)].reshape(YN * ROWS, 128)
+                values = jnp.concatenate([vbuf[first + i] for i in range(YN)], axis=1)
+            else:
+                slots = [slot(row, (y + step) % YN) for step in steps]
+                keys = jnp.concatenate([kbuf[s] for s in slots], axis=0)
+                values = jnp.concatenate([vbuf[s] for s in slots], axis=1)
+            scores = dot(keys, qt[part])
+            if diagonal:
+                key_at = lax.broadcasted_iota(jnp.int32, scores.shape, 0)
+                query_at = lax.broadcasted_iota(jnp.int32, scores.shape, 1) % ROWS + y * ROWS
+                scores = jnp.where(query_at >= key_at, scores, -1e30)
+                new = jnp.max(scores, axis=0, keepdims=True)
+                weights = jnp.exp(scores - new)
+                total[part] = jnp.sum(weights, axis=0, keepdims=True)
+                att[part] = dot(values, weights.astype(BF))
+            else:
+                old = peak[part]
                 new = jnp.maximum(old, jnp.max(scores, axis=0, keepdims=True))
                 weights = jnp.exp(scores - new)
                 fade = jnp.exp(old - new)
-                total[chunk] = total[chunk] * fade + jnp.sum(weights, axis=0, keepdims=True)
-                att[chunk] = att[chunk] * fade + dot(values, weights.astype(BF))
-                peak[chunk] = new
-                return carry
-
-            lax.fori_loop(0, 4, one, 0)
+                total[part] = total[part] * fade + jnp.sum(weights, axis=0, keepdims=True)
+                att[part] = att[part] * fade + dot(values, weights.astype(BF))
+            peak[part] = new
 
         if ok is None:
-            all_chunks()
+            run()
         else:
-            pl.when(ok)(all_chunks)
-
-    plus_keys(1)
-    minus_keys(1)
-    peak[...] = jnp.full_like(peak, -1e30)
-    total[...] = jnp.zeros_like(total)
-    att[...] = jnp.zeros_like(att)
-    finish_v(z, always)
-    attend(z, None, True)
-
-    relay_v(*row_plus(1))
-    relay_v(*row_minus(1))
-    plus(vbuf, vsem, 2, y)
-    minus(vbuf, vsem, 2, y)
-    spread_v(*row_plus(2))
-    spread_v(*row_minus(2))
-
-    for step in (1, 3, 2):
-        col = (y + step) % YN
-        arrived(crow.at[col], crsem.at[col])
-    all_a = crow[0, 0:1, :]
-    all_s = crow[0, 1:2, :]
-    for col in range(1, YN):
-        all_s = crow[col, 0:1, :] * all_s + crow[col, 1:2, :]
-        all_a = crow[col, 0:1, :] * all_a
-    ctot[z, 0:1, :] = all_a
-    ctot[z, 1:2, :] = all_s
-    send(ctot.at[z], ctot.at[z], ctsem.at[z], when=has_up, sp=up)
-    send(ctot.at[z], ctot.at[z], ctsem.at[z], when=goes_down, sp=down)
-
-    def plus_carry(d):
-        row, ok = row_plus(d)
+            pl.when(ok)(run)
+
+    fillers = []
+
+    def filler():
+        if fillers:
+            fillers.pop(0)()
+
+    def ready(row, ok, **how):
+        for part in range(4):
+            fillers.append(lambda part=part: attend(row, ok, part, **how))
+
+    def run(*ops):
+        for op in ops:
+            op()
+            filler()
+
+    def row_carry():
+        for step in (1, 3, 2):
+            col = (y + step) % YN
+            arrived(crow.at[col], crsem.at[col])
+        all_a = crow[0, 0:1, :]
+        all_s = crow[0, 1:2, :]
+        for col in range(1, YN):
+            all_s = crow[col, 0:1, :] * all_s + crow[col, 1:2, :]
+            all_a = crow[col, 0:1, :] * all_a
+        ctot[z, 0:1, :] = all_a
+        ctot[z, 1:2, :] = all_s
+        send(ctot.at[z], ctot.at[z], ctsem.at[z], when=has_up, sp=up)
+        send_down(ctot, ctsem, z, goes_down)
+
+    def carry(n):
+        row, ok = row_plus(n)
         arrived(ctot.at[row], ctsem.at[row], ok)
-        if d < FWD:
+        if n < FWD:
             send(ctot.at[row], ctot.at[row], ctsem.at[row], when=ok & has_up, sp=up)
-
-    def minus_carry(e):
-        row = (z + e) % ZN
-        ok = row <= BACK - 1
-        arrived(ctot.at[row], ctsem.at[row], ok)
-        if e < BACK:
-            send(ctot.at[row], ctot.at[row], ctsem.at[row], when=ok, sp=down)
-
-    plus(kbuf, ksem, 2, y)
-    minus(kbuf, ksem, 2, y)
-    plus_keys(2)
-    minus_keys(2)
-    finish_v(*row_plus(1))
-    finish_v(*row_minus(1))
-    attend(*row_plus(1), False)
-    plus_carry(1)
-    minus_carry(1)
-    relay_v(*row_plus(2))
-    relay_v(*row_minus(2))
-    plus(vbuf, vsem, 3, y)
-    minus(vbuf, vsem, 3, y)
-    spread_v(*row_plus(3))
-    spread_v(*row_minus(3))
-    plus(kbuf, ksem, 3, y)
-    minus(kbuf, ksem, 3, y)
-    attend(*row_minus(1), False)
-    plus_carry(2)
-    minus_carry(2)
-    plus_keys(3)
-    minus_keys(3)
-    finish_v(*row_plus(2))
-    finish_v(*row_minus(2))
-    attend(*row_plus(2), False)
-    plus_carry(3)
-    minus_carry(3)
-    relay_v(*row_plus(3))
-    relay_v(*row_minus(3))
-    plus(vbuf, vsem, 4, y)
-    spread_v(*row_plus(4))
-    plus(kbuf, ksem, 4, y)
-    attend(*row_minus(2), False)
-    plus_carry(4)
+        if n <= BACK:
+            row = (z + n) % ZN
+            ok = row <= BACK - 1
+            arrived(ctot.at[row], ctsem.at[row], ok)
+            if n < BACK:
+                send_down(ctot, ctsem, row, ok)
 
     def fold_total(row, s):
         return ctot[row, 0:1, :] * s + ctot[row, 1:2, :]
@@ -399,21 +414,46 @@
     def fold_row(col, s):
         return crow[col, 0:1, :] * s + crow[col, 1:2, :]
 
-    carry_in = lax.fori_loop(0, z, fold_total, jnp.zeros((1, 512), F32))
-    carry_in = lax.fori_loop(0, y, fold_row, carry_in)
-    recur_out = (states[...] + decs[...] * carry_in).astype(BF)
-    l_wor.wait()
+    def recur_output():
+        carry_in = lax.fori_loop(0, z, fold_total, jnp.zeros((1, 512), F32))
+        carry_in = lax.fori_loop(0, y, fold_row, carry_in)
+        rout[...] = (states[...] + decs[...] * carry_in).astype(BF)
+        l_wor.wait()
+
+    def recur_project(n):
+        mbuf[n] = dot(rout[...], wor[:, n * 512 : n * 512 + 512])
+
+    finish_v(z, always)
+    ready(z, None, diagonal=True)
+    run(key(1, 1, 1), key(1, 1, 3), key(1, 1, 2))
+    run(lambda: v_plus(3), lambda: v_minus(3))
+    run(lambda: relay_v(*row_plus(2)), lambda: relay_v(*row_minus(1)), lambda: finish_v(*row_plus(1)))
+    ready(*row_plus(1))
+    run(key(-1, 1, 0), key(-1, 1, 1), key(1, 2, 0), key(-1, 1, 3), key(1, 2, 1), row_carry)
+    run(key(-1, 1, 2), key(1, 2, 3), key(1, 2, 2), lambda: relay_v(*row_minus(2)))
+    run(lambda: v_plus(4), lambda: relay_v(*row_plus(3)), lambda: finish_v(*row_plus(2)))
+    ready(*row_plus(2))
+    run(lambda: finish_v(*row_minus(1)), lambda: relay_v(*row_minus(3)))
+    ready(*row_minus(1))
+    run(lambda: carry(1), key(-1, 2, 0), key(-1, 2, 1), key(1, 3, 0), key(-1, 2, 3), key(1, 3, 1))
+    run(key(-1, 2, 2), key(1, 3, 3), lambda: carry(2), key(1, 3, 2), lambda: finish_v(*row_minus(2)))
+    ready(*row_minus(2))
+    run(lambda: relay_v(*row_plus(4)), lambda: finish_v(*row_plus(3)), lambda: finish_v(*row_minus(3)))
+    ready(*row_plus(3))
+    run(lambda: carry(3), key(-1, 3, 0), key(-1, 3, 1), key(-1, 3, 3), lambda: carry(4), key(-1, 3, 2))
+    fillers.append(recur_output)
     for n in range(4):
-        mbuf[n] = dot(recur_out, wor[:, n * 512 : n * 512 + 512])
-
-    finish_v(*row_plus(3))
-    finish_v(*row_minus(3))
-    attend(*row_plus(3), False)
-    relay_v(*row_plus(4))
-    attend(*row_minus(3), False)
-    plus_keys(4)
-    finish_v(*row_plus(4))
-    attend(*row_plus(4), False)
+        fillers.append(lambda n=n: recur_project(n))
+    ready(*row_minus(3))
+    run(lambda: finish_v(*row_plus(4)), key(1, 4, 0), key(1, 4, 1))
+    ready(*row_plus(4), steps=(0, 1))
+    run(key(1, 4, 3))
+    while len(fillers) > 1:
+        filler()
+    run(key(1, 4, 2))
+    ready(*row_plus(4), steps=(3, 2))
+    while fillers:
+        filler()
 
     pieces = []
     for h in range(4):
@@ -440,14 +480,12 @@
     scale = lax.rsqrt(power / D + EPS)
     for n in range(4):
         cols = slice(n * 512, n * 512 + 512)
-        outv[:, cols] = (mrecv[n] * scale * ogain[:, cols]).astype(BF)
-    last = load(outv, out_h)
+        out_h[:, cols] = (mrecv[n] * scale * ogain[:, cols]).astype(BF)
     for copy, when in sends:
         if when is None:
             copy.wait_send()
         else:
             pl.when(when)(lambda copy=copy: copy.wait_send())
-    last.wait()
 
 
 def body(
@@ -459,7 +497,7 @@
     dma = pltpu.SemaphoreType.DMA
     scratch = [
         vmem((2, ROWS, HALF), BF), vmem((2, 1, HALF), F32), vmem((D, 512), BF), vmem((4, 512), F32),
-        vmem((8, 64, 64), BF), vmem((8, 64, 64), BF), vmem((1, 512), F32), vmem((ROWS, 8), F32),
+        vmem((8, 64, 64), BF), vmem((8, 64, 64), BF), vmem((1, 512), F32), vmem((8, ROWS), F32),
         vmem((D, 512), BF), vmem((D, 256), BF), vmem((1, 4), F32), vmem((1, 128), F32),
         vmem((512, D), BF), vmem((512, D), BF), vmem((1, D), F32),
         vmem((2, ROWS, HALF), BF), vmem((ROWS, 1280), F32),
@@ -468,14 +506,15 @@
         vmem((4, 128, 256), BF), vmem((4, 128, 256), F32), vmem((4, 1, 256), F32), vmem((4, 1, 256), F32),
         vmem((4, 128, 256), BF),
         vmem((YN, 2, 512), F32), vmem((ZN, 2, 512), F32), vmem((ROWS, 512), F32), vmem((ROWS, 512), F32),
-        vmem((4, ROWS, 512), F32), vmem((4, 64, 512), F32), vmem((64, D), BF),
+        vmem((4, ROWS, 512), F32), vmem((4, 64, 512), F32), vmem((ROWS, 512), BF),
         dma((24,)), dma((NSEND,)), dma, dma((SP,)), dma((SP,)), dma, dma((YN,)), dma((ZN,)), dma((4,)),
+        pltpu.SemaphoreType.REGULAR,
     ]
     return pl.pallas_call(
         kernel,
-        out_shape=jax.ShapeDtypeStruct((64, D), BF),
+        out_shape=pltpu.VMEM((64, D), BF),
         in_specs=[any_] * 16,
-        out_specs=any_,
+        out_specs=pl.BlockSpec(memory_space=pltpu.VMEM),
         scratch_shapes=scratch,
         compiler_params=pltpu.CompilerParams(
             collective_id=0, has_side_effects=True, vmem_limit_bytes=60 * 1024 * 1024
@@ -483,7 +522,7 @@
         name="layer",
     )(
         tokens, norm_gain.reshape(2, 1, HALF), w_recur_in, conv_weight, w_gate_decay, w_gate_input,
-        decay_base.reshape(1, -1), extra_decay, w_query, w_key, w_value, mix_lambda.reshape(1, -1),
+        decay_base.reshape(1, -1), extra_decay.T, w_query, w_key, w_value, mix_lambda.reshape(1, -1),
         head_gain.reshape(1, -1), w_out_recur, w_out_attend, out_gain.reshape(1, -1),
     )
 

time: 47.5 us -> 49.2 us (1.036)
  Pallas kernels: 44.3 us -> 48.4 us
  local copies, waits for them, and re-layouts: 3.08 us -> 0.71 us
    pallas_call x1, Pallas kernels: 44.3 us -> 48.4 us  [body(): pl.pallas_call(kernel, out_shape=pltpu.VMEM((64, D), BF), in_specs=[any_]...]
    unnamed x2 -> x1, local copies, waits for them, and re-layouts: 3.08 us -> 0.71 us
where the time goes in v2:
time: 49.2 us; the launch traced here: 49.1 us
  Pallas kernels  48.4 us (98%)
  local copies, waits for them, and re-layouts  0.71 us (1%)
    pallas_call x1, Pallas kernels, body(): pl.pallas_call(kernel, out_shape=pltpu.VMEM((64, D), BF), in_specs=[any_]...  48.4 us

profile of v2, /device:TPU:193, one launch (start us, length us, event | category | flops | bytes accessed | tf_op | source)
XLA Modules:
  0.0 49.1 jit_solution(1993900785837973218)
XLA Ops:
  0.0 48.4 %layer.1 = bf16[64,2048]{1,0:T(8,128)(2,1)S(1)} custom-call(bf16[128,1024]{1,0:T(8,128)(2,1)} %tok_h.1, f32[2,1,1024]{2,1,0:T(1,128)} %bitcast.6, bf16[2048,512]{1,0:T(8,128)(2,1)} %wr_h.1, f32[4,512]{1,0:T(4,128)} %cw_h.1, bf16[8,64,64]{2,1,0:T(8,128)(2,1)} %wgd_h.1, bf16[8,64,64]{2,1,0:T(8,128)(2,1)} %wgi_h.1, f32[1,512]{1,0:T(1,128)} %bitcast.9, ...), custom_call_target="tpu_custom_call" | custom-call | tf_op jit(solution)/shard_map/layer/pallas_call | solution.py:513
  48.4 0.7 %copy.18 = bf16[64,2048]{1,0:T(8,128)(2,1)} copy(bf16[64,2048]{1,0:T(8,128)(2,1)S(1)} %layer.1) | data formatting | bytes 524288

commit v3 on v2

--- a/solution.py
+++ b/solution.py
@@ -40,7 +40,7 @@
     tok, gain, wr, cw, wgd, wgi, base, extra, wq, wkv, lam, hgain, wor, woa, ogain,
     scaled, acc, kbuf, vbuf, rin, halo, xext, qt, att, peak, total, gates,
     crow, ctot, decs, states, mbuf, mrecv, rout,
-    lsem, ssem, tsem, ksem, vsem, hsem, crsem, ctsem, msem, insem,
+    lsem, ssem, tsem, ksem, vsem, hsem, crsem, ctsem, msem,
 ):
     sp = lax.axis_index("sp")
     c = lax.axis_index("tp")
@@ -84,11 +84,13 @@
         )
     has_up = z < ZN - 1
     has_down = z > 0
+    around = (z == 0) | (z == ZN - 1)
     corner_up = (y == YN - 1) & has_up
     corner_down = (y == 0) & has_down
     greeted = 4
     for when, target in (
-        (has_up, (z + 1) * YN + y), (has_down, (z - 1) * YN + y), (corner_up, sp + 1), (corner_down, sp - 1)
+        (has_up, (z + 1) * YN + y), (has_down, (z - 1) * YN + y), (around, (ZN - 1 - z) * YN + y),
+        (corner_up, sp + 1), (corner_down, sp - 1),
     ):
         near = jnp.where(when, target, sp)
 
@@ -99,10 +101,11 @@
         greeted = greeted + when.astype(jnp.int32)
 
     sends = []
+    numbers = iter(range(NSEND))
 
     def send(src, dst, rsem, when=None, **target):
         copy = pltpu.make_async_remote_copy(
-            src_ref=src, dst_ref=dst, send_sem=ssem.at[len(sends)], recv_sem=rsem,
+            src_ref=src, dst_ref=dst, send_sem=ssem.at[next(numbers)], recv_sem=rsem,
             device_id=target, device_id_type=MESH,
         )
         sends.append((copy, when))
@@ -124,21 +127,12 @@
     up = ((z + 1) % ZN) * YN + y
     down = ((z + ZN - 1) % ZN) * YN + y
 
-    def pass_in(k):
-        @pl.when(z == ZN - 1 - k)
-        def _():
-            if k > 0:
-                pl.semaphore_wait(insem, 1)
-            if k < ZN - 1:
-                pl.semaphore_signal(insem, inc=1, device_id={"sp": down}, device_id_type=MESH)
-
     def beside(step):
         return z * YN + (y + step + YN) % YN
 
     l_tok.wait()
     pl.semaphore_wait(barrier, greeted)
     send(tok.at[c], tok.at[c], tsem, tp=1 - c)
-    pass_in(0)
     l_wor = load(wor_h, wor)
     l_woa = load(woa_h, woa)
 
@@ -173,23 +167,17 @@
         send(buf.at[s], buf.at[s], sem.at[s], when=when, sp=to)
 
     goes_down = z <= BACK - 1
-    postponed = []
 
     def send_down(buf, sem, at, when):
-        send(buf.at[at], buf.at[at], sem.at[at], when=when & has_down, sp=down)
-        wrap = lambda: send(buf.at[at], buf.at[at], sem.at[at], when=when & (z == 0), sp=down)
-        if postponed is None:
-            wrap()
-        else:
-            postponed.append(wrap)
+        send(buf.at[at], buf.at[at], sem.at[at], when=when, sp=down)
 
     def forward_own(buf, sem, col):
         send_block(buf, sem, z, col, up, has_up)
         send_down(buf, sem, slot(z, col), goes_down)
 
+    for step in (1, 3):
+        send(kbuf.at[sp], kbuf.at[sp], ksem.at[sp], sp=beside(step))
     forward_own(vbuf, vsem, y)
-    for step in (1, 3, 2):
-        send(kbuf.at[sp], kbuf.at[sp], ksem.at[sp], sp=beside(step))
     forward_own(kbuf, ksem, y)
 
     def plus(buf, sem, d, col):
@@ -226,6 +214,22 @@
         arrived(vbuf.at[s], vsem.at[s], ok)
         send(vbuf.at[s], vbuf.at[s], vsem.at[s], when=ok, sp=beside(way))
 
+    def keys_beside():
+        way = 2 * (z % 2) - 1
+        for turn in (-way, way):
+            col = (y + turn + YN) % YN
+            s = slot(z, col)
+            arrived(kbuf.at[s], ksem.at[s])
+            if turn is not way:
+                send(kbuf.at[s], kbuf.at[s], ksem.at[s], sp=beside(way))
+            forward_own(kbuf, ksem, col)
+
+    def keys_across():
+        col = (y + 2) % YN
+        s = slot(z, col)
+        arrived(kbuf.at[s], ksem.at[s])
+        forward_own(kbuf, ksem, col)
+
     def finish_v(row, ok):
         way = 1 - 2 * (row % 2)
         for col in ((y + way + YN) % YN, (y + 2) % YN):
@@ -241,7 +245,6 @@
     send(rin.at[pl.ds(ROWS - 16, 16)], halo, hsem, when=sp < SP - 1, sp=(sp + 1) % SP)
     xext[pl.ds(8, ROWS), :] = recur.astype(F32)
 
-    pass_in(1)
 
     def v_plus(d):
         plus(vbuf, vsem, d, y)
@@ -261,17 +264,10 @@
         qt[h // 2, 0:64, lanes] = turned[0:64]
         qt[2 + h // 2, 64:128, lanes] = turned[64:128]
 
-    pass_in(2)
+
+    keys_beside()
     v_plus(1)
-
-    for step in (1, 3, 2):
-        col = (y + step) % YN
-        s = slot(z, col)
-        arrived(kbuf.at[s], ksem.at[s])
-        forward_own(kbuf, ksem, col)
-    plus(kbuf, ksem, 1, y)
-    pass_in(3)
-    relay_v(z, always)
+    v_minus(1)
 
     for copy in l_small:
         copy.wait()
@@ -312,29 +308,27 @@
         crow[y, 0:1, cols] = a[ROWS - 1 : ROWS]
         crow[y, 1:2, cols] = b[ROWS - 1 : ROWS]
 
-    pass_in(4)
+
     recur_columns(0)
-    v_plus(2)
-    v_minus(1)
-    pass_in(5)
     recur_columns(1)
+    plus(kbuf, ksem, 1, y)
+    minus(kbuf, ksem, 1, y)
+    relay_v(z, always)
     recur_columns(2)
-    v_minus(2)
-    pass_in(6)
     recur_columns(3)
     for step in (1, 3, 2):
         send(crow.at[y], crow.at[y], crsem.at[y], sp=beside(step))
-    pass_in(7)
-    for wrap in postponed:
-        wrap()
-    postponed = None
+    keys_across()
+    v_plus(2)
+    v_minus(2)
     relay_v(*row_plus(1))
+    relay_v(*row_minus(1))
 
     def key(sign, n, step):
         move = plus if sign > 0 else minus
         return lambda: move(kbuf, ksem, n, (y + step) % YN)
 
-    def attend(row, ok, part, diagonal=False, steps=None):
+    def attend(row, ok, parts, diagonal=False, steps=None):
         def run():
             if steps is None:
                 first = row * YN
@@ -344,23 +338,24 @@
                 slots = [slot(row, (y + step) % YN) for step in steps]
                 keys = jnp.concatenate([kbuf[s] for s in slots], axis=0)
                 values = jnp.concatenate([vbuf[s] for s in slots], axis=1)
-            scores = dot(keys, qt[part])
-            if diagonal:
-                key_at = lax.broadcasted_iota(jnp.int32, scores.shape, 0)
-                query_at = lax.broadcasted_iota(jnp.int32, scores.shape, 1) % ROWS + y * ROWS
-                scores = jnp.where(query_at >= key_at, scores, -1e30)
-                new = jnp.max(scores, axis=0, keepdims=True)
-                weights = jnp.exp(scores - new)
-                total[part] = jnp.sum(weights, axis=0, keepdims=True)
-                att[part] = dot(values, weights.astype(BF))
-            else:
-                old = peak[part]
-                new = jnp.maximum(old, jnp.max(scores, axis=0, keepdims=True))
-                weights = jnp.exp(scores - new)
-                fade = jnp.exp(old - new)
-                total[part] = total[part] * fade + jnp.sum(weights, axis=0, keepdims=True)
-                att[part] = att[part] * fade + dot(values, weights.astype(BF))
-            peak[part] = new
+            all_scores = [dot(keys, qt[part]) for part in parts]
+            for part, scores in zip(parts, all_scores):
+                if diagonal:
+                    key_at = lax.broadcasted_iota(jnp.int32, scores.shape, 0)
+                    query_at = lax.broadcasted_iota(jnp.int32, scores.shape, 1) % ROWS + y * ROWS
+                    scores = jnp.where(query_at >= key_at, scores, -1e30)
+                    new = jnp.max(scores, axis=0, keepdims=True)
+                    weights = jnp.exp(scores - new)
+                    total[part] = jnp.sum(weights, axis=0, keepdims=True)
+                    att[part] = dot(values, weights.astype(BF))
+                else:
+                    old = peak[part]
+                    new = jnp.maximum(old, jnp.max(scores, axis=0, keepdims=True))
+                    weights = jnp.exp(scores - new)
+                    fade = jnp.exp(old - new)
+                    total[part] = total[part] * fade + jnp.sum(weights, axis=0, keepdims=True)
+                    att[part] = att[part] * fade + dot(values, weights.astype(BF))
+                peak[part] = new
 
         if ok is None:
             run()
@@ -374,8 +369,8 @@
             fillers.pop(0)()
 
     def ready(row, ok, **how):
-        for part in range(4):
-            fillers.append(lambda part=part: attend(row, ok, part, **how))
+        for parts in ((0, 1, 2, 3),) if "steps" in how else ((0, 1), (2, 3)):
+            fillers.append(lambda parts=parts: attend(row, ok, parts, **how))
 
     def run(*ops):
         for op in ops:
@@ -423,37 +418,45 @@
     def recur_project(n):
         mbuf[n] = dot(rout[...], wor[:, n * 512 : n * 512 + 512])
 
+    def drain():
+        while sends:
+            copy, when = sends.pop(0)
+            if when is None:
+                copy.wait_send()
+            else:
+                pl.when(when)(lambda copy=copy: copy.wait_send())
+
     finish_v(z, always)
     ready(z, None, diagonal=True)
-    run(key(1, 1, 1), key(1, 1, 3), key(1, 1, 2))
+    run(key(1, 1, 1), key(-1, 1, 1), key(1, 1, 3), key(-1, 1, 3))
+    run(key(1, 2, 0), key(-1, 2, 0), key(1, 1, 2), key(-1, 1, 2))
     run(lambda: v_plus(3), lambda: v_minus(3))
-    run(lambda: relay_v(*row_plus(2)), lambda: relay_v(*row_minus(1)), lambda: finish_v(*row_plus(1)))
+    run(lambda: relay_v(*row_plus(2)), lambda: relay_v(*row_minus(2)), lambda: finish_v(*row_plus(1)))
     ready(*row_plus(1))
-    run(key(-1, 1, 0), key(-1, 1, 1), key(1, 2, 0), key(-1, 1, 3), key(1, 2, 1), row_carry)
-    run(key(-1, 1, 2), key(1, 2, 3), key(1, 2, 2), lambda: relay_v(*row_minus(2)))
-    run(lambda: v_plus(4), lambda: relay_v(*row_plus(3)), lambda: finish_v(*row_plus(2)))
+    run(lambda: finish_v(*row_minus(1)))
+    ready(*row_minus(1))
+    run(row_carry, key(1, 2, 1), key(-1, 2, 1), key(1, 2, 3), key(-1, 2, 3))
+    run(key(1, 3, 0), key(-1, 3, 0), key(1, 2, 2), key(-1, 2, 2))
+    run(lambda: v_plus(4), lambda: relay_v(*row_plus(3)), lambda: relay_v(*row_minus(3)))
+    run(lambda: finish_v(*row_plus(2)))
     ready(*row_plus(2))
-    run(lambda: finish_v(*row_minus(1)), lambda: relay_v(*row_minus(3)))
-    ready(*row_minus(1))
-    run(lambda: carry(1), key(-1, 2, 0), key(-1, 2, 1), key(1, 3, 0), key(-1, 2, 3), key(1, 3, 1))
-    run(key(-1, 2, 2), key(1, 3, 3), lambda: carry(2), key(1, 3, 2), lambda: finish_v(*row_minus(2)))
+    run(lambda: carry(1), lambda: finish_v(*row_minus(2)))
     ready(*row_minus(2))
-    run(lambda: relay_v(*row_plus(4)), lambda: finish_v(*row_plus(3)), lambda: finish_v(*row_minus(3)))
+    run(key(1, 3, 1), key(-1, 3, 1), lambda: carry(2), key(1, 3, 3), key(-1, 3, 3))
+    run(key(1, 4, 0), key(1, 3, 2), key(-1, 3, 2))
+    run(lambda: relay_v(*row_plus(4)), lambda: finish_v(*row_plus(3)))
     ready(*row_plus(3))
-    run(lambda: carry(3), key(-1, 3, 0), key(-1, 3, 1), key(-1, 3, 3), lambda: carry(4), key(-1, 3, 2))
+    run(lambda: carry(3), lambda: finish_v(*row_minus(3)))
+    ready(*row_minus(3))
+    run(key(1, 4, 1), lambda: carry(4), key(1, 4, 3), drain, lambda: finish_v(*row_plus(4)))
     fillers.append(recur_output)
     for n in range(4):
         fillers.append(lambda n=n: recur_project(n))
-    ready(*row_minus(3))
-    run(lambda: finish_v(*row_plus(4)), key(1, 4, 0), key(1, 4, 1))
-    ready(*row_plus(4), steps=(0, 1))
-    run(key(1, 4, 3))
-    while len(fillers) > 1:
-        filler()
-    run(key(1, 4, 2))
-    ready(*row_plus(4), steps=(3, 2))
     while fillers:
         filler()
+    key(1, 4, 2)()
+    attend(*row_plus(4), (0, 1), steps=(0, 1, 3, 2))
+    attend(*row_plus(4), (2, 3), steps=(0, 1, 3, 2))
 
     pieces = []
     for h in range(4):
@@ -481,11 +484,7 @@
     for n in range(4):
         cols = slice(n * 512, n * 512 + 512)
         out_h[:, cols] = (mrecv[n] * scale * ogain[:, cols]).astype(BF)
-    for copy, when in sends:
-        if when is None:
-            copy.wait_send()
-        else:
-            pl.when(when)(lambda copy=copy: copy.wait_send())
+    drain()
 
 
 def body(
@@ -508,7 +507,6 @@
         vmem((YN, 2, 512), F32), vmem((ZN, 2, 512), F32), vmem((ROWS, 512), F32), vmem((ROWS, 512), F32),
         vmem((4, ROWS, 512), F32), vmem((4, 64, 512), F32), vmem((ROWS, 512), BF),
         dma((24,)), dma((NSEND,)), dma, dma((SP,)), dma((SP,)), dma, dma((YN,)), dma((ZN,)), dma((4,)),
-        pltpu.SemaphoreType.REGULAR,
     ]
     return pl.pallas_call(
         kernel,

time: 49.2 us -> 37.8 us (0.77); the launches traced: 49.1 us -> 37.2 us
  Pallas kernels: 48.4 us -> 36.5 us
    pallas_call x1, Pallas kernels: 48.4 us -> 36.5 us  [body(): pl.pallas_call(kernel, out_shape=pltpu.VMEM((64, D), BF), in_specs=[any_]...]
where the time goes in v3:
time: 37.8 us; the launch traced here: 37.2 us
  Pallas kernels  36.5 us (97%)
  local copies, waits for them, and re-layouts  0.71 us (2%)
    pallas_call x1, Pallas kernels, body(): pl.pallas_call(kernel, out_shape=pltpu.VMEM((64, D), BF), in_specs=[any_]...  36.5 us

profile of v3, /device:TPU:193, one launch (start us, length us, event | category | flops | bytes accessed | tf_op | source)
XLA Modules:
  0.0 37.2 jit_solution(5145543512586866369)
XLA Ops:
  0.0 36.5 %layer.1 = bf16[64,2048]{1,0:T(8,128)(2,1)S(1)} custom-call(bf16[128,1024]{1,0:T(8,128)(2,1)} %tok_h.1, f32[2,1,1024]{2,1,0:T(1,128)} %bitcast.6, bf16[2048,512]{1,0:T(8,128)(2,1)} %wr_h.1, f32[4,512]{1,0:T(4,128)} %cw_h.1, bf16[8,64,64]{2,1,0:T(8,128)(2,1)} %wgd_h.1, bf16[8,64,64]{2,1,0:T(8,128)(2,1)} %wgi_h.1, f32[1,512]{1,0:T(1,128)} %bitcast.9, ...), custom_call_target="tpu_custom_call" | custom-call | tf_op jit(solution)/shard_map/layer/pallas_call | solution.py:511
  36.5 0.7 %copy.18 = bf16[64,2048]{1,0:T(8,128)(2,1)} copy(bf16[64,2048]{1,0:T(8,128)(2,1)S(1)} %layer.1) | data formatting | bytes 524288

commit v4 on v3

--- a/solution.py
+++ b/solution.py
@@ -18,8 +18,8 @@
 SP = ZN * YN
 RATE = 8.0
 EPS = 1e-06
-FWD = 4
-BACK = 3
+FWD = 3
+BACK = 4
 NSEND = 144
 
 
@@ -40,7 +40,7 @@
     tok, gain, wr, cw, wgd, wgi, base, extra, wq, wkv, lam, hgain, wor, woa, ogain,
     scaled, acc, kbuf, vbuf, rin, halo, xext, qt, att, peak, total, gates,
     crow, ctot, decs, states, mbuf, mrecv, rout,
-    lsem, ssem, tsem, ksem, vsem, hsem, crsem, ctsem, msem,
+    lsem, ssem, tsem, ksem, vsem, hsem, crsem, ctsem, msem, known,
 ):
     sp = lax.axis_index("sp")
     c = lax.axis_index("tp")
@@ -130,6 +130,11 @@
     def beside(step):
         return z * YN + (y + step + YN) % YN
 
+    def tell(n, distance):
+        pl.semaphore_signal(
+            known.at[n], inc=1, device_id={"sp": ((z + distance) % ZN) * YN + y}, device_id_type=MESH
+        )
+
     l_tok.wait()
     pl.semaphore_wait(barrier, greeted)
     send(tok.at[c], tok.at[c], tsem, tp=1 - c)
@@ -144,6 +149,8 @@
         return jnp.sum(x * x, axis=1, keepdims=True)
 
     squares = scale_half(c)
+    tell(0, 1)
+    tell(1, ZN - 1)
     for copy in l_own:
         copy.wait()
     acc[:, 0:256] = dot(scaled[c], wkv[own_rows, :])
@@ -175,7 +182,7 @@
         send_block(buf, sem, z, col, up, has_up)
         send_down(buf, sem, slot(z, col), goes_down)
 
-    for step in (1, 3):
+    for step in (1, 3, 2):
         send(kbuf.at[sp], kbuf.at[sp], ksem.at[sp], sp=beside(step))
     forward_own(vbuf, vsem, y)
     forward_own(kbuf, ksem, y)
@@ -203,10 +210,12 @@
         row = (z + e) % ZN
         return row, (row <= BACK - 1) & (z > row)
 
-    def spread_v(row, ok):
+    def spread_v(row, ok, across=False):
         way = 1 - 2 * (row % 2)
         send_block(vbuf, vsem, row, y, beside(way), ok)
         send_block(vbuf, vsem, row, y, beside(-way), ok)
+        if across:
+            send_block(vbuf, vsem, row, y, beside(2), ok)
 
     def relay_v(row, ok):
         way = 1 - 2 * (row % 2)
@@ -215,13 +224,10 @@
         send(vbuf.at[s], vbuf.at[s], vsem.at[s], when=ok, sp=beside(way))
 
     def keys_beside():
-        way = 2 * (z % 2) - 1
-        for turn in (-way, way):
-            col = (y + turn + YN) % YN
+        for step in (1, 3):
+            col = (y + step) % YN
             s = slot(z, col)
             arrived(kbuf.at[s], ksem.at[s])
-            if turn is not way:
-                send(kbuf.at[s], kbuf.at[s], ksem.at[s], sp=beside(way))
             forward_own(kbuf, ksem, col)
 
     def keys_across():
@@ -230,9 +236,12 @@
         arrived(kbuf.at[s], ksem.at[s])
         forward_own(kbuf, ksem, col)
 
-    def finish_v(row, ok):
+    def finish_v(row, ok, across=False):
         way = 1 - 2 * (row % 2)
-        for col in ((y + way + YN) % YN, (y + 2) % YN):
+        cols = [(y + way + YN) % YN, (y + 2) % YN]
+        if across:
+            cols.append((y - way + YN) % YN)
+        for col in cols:
             s = slot(row, col)
             arrived(vbuf.at[s], vsem.at[s], ok)
 
@@ -248,11 +257,11 @@
 
     def v_plus(d):
         plus(vbuf, vsem, d, y)
-        spread_v(*row_plus(d))
+        spread_v(*row_plus(d), across=d == FWD)
 
     def v_minus(e):
         minus(vbuf, vsem, e, y)
-        spread_v(*row_minus(e))
+        spread_v(*row_minus(e), across=e == BACK)
 
     l_q.wait()
     query = ((acc[:, 768:1280] + dot(scaled[1 - c], wq[other_rows, :])) * inverse).astype(BF)
@@ -265,9 +274,59 @@
         qt[2 + h // 2, 64:128, lanes] = turned[64:128]
 
 
-    keys_beside()
+    def attend(row, ok, steps=(), first_of_all=False, earlier=False):
+        def run():
+            if steps:
+                slots = [slot(row, (y + step) % YN) for step in steps]
+                keys = jnp.concatenate([kbuf[s] for s in slots], axis=0)
+                values = jnp.concatenate([vbuf[s] for s in slots], axis=1)
+            else:
+                first = row * YN
+                keys = kbuf[pl.ds(first, YN)].reshape(YN * ROWS, 128)
+                values = jnp.concatenate([vbuf[first + i] for i in range(YN)], axis=1)
+            all_scores = [dot(keys, qt[part]) for part in range(4)]
+            for part, scores in enumerate(all_scores):
+                if first_of_all:
+                    key_at = lax.broadcasted_iota(jnp.int32, scores.shape, 0)
+                    query_at = lax.broadcasted_iota(jnp.int32, scores.shape, 1) % ROWS
+                    scores = jnp.where(query_at >= key_at, scores, -1e30)
+                    new = jnp.max(scores, axis=0, keepdims=True)
+                    weights = jnp.exp(scores - new)
+                    total[part] = jnp.sum(weights, axis=0, keepdims=True)
+                    att[part] = dot(values, weights.astype(BF))
+                else:
+                    if earlier:
+                        scores = jnp.concatenate(
+                            [
+                                jnp.where((y + step) % YN < y, scores[n * ROWS : n * ROWS + ROWS], -1e30)
+                                for n, step in enumerate(steps)
+                            ],
+                            axis=0,
+                        )
+                    old = peak[part]
+                    new = jnp.maximum(old, jnp.max(scores, axis=0, keepdims=True))
+                    weights = jnp.exp(scores - new)
+                    fade = jnp.exp(old - new)
+                    total[part] = total[part] * fade + jnp.sum(weights, axis=0, keepdims=True)
+                    att[part] = att[part] * fade + dot(values, weights.astype(BF))
+                peak[part] = new
+
+        if ok is None:
+            run()
+        else:
+            pl.when(ok)(run)
+
+    attend(z, None, steps=(0,), first_of_all=True)
     v_plus(1)
     v_minus(1)
+    keys_beside()
+    plus(kbuf, ksem, 1, y)
+    minus(kbuf, ksem, 1, y)
+    relay_v(z, always)
+    pl.semaphore_wait(known.at[0], 1)
+    pl.semaphore_wait(known.at[1], 1)
+    tell(2, 2)
+    tell(3, ZN - 2)
 
     for copy in l_small:
         copy.wait()
@@ -311,71 +370,19 @@
 
     recur_columns(0)
     recur_columns(1)
-    plus(kbuf, ksem, 1, y)
-    minus(kbuf, ksem, 1, y)
-    relay_v(z, always)
+    keys_across()
+    v_plus(2)
+    v_minus(2)
     recur_columns(2)
     recur_columns(3)
     for step in (1, 3, 2):
         send(crow.at[y], crow.at[y], crsem.at[y], sp=beside(step))
-    keys_across()
-    v_plus(2)
-    v_minus(2)
     relay_v(*row_plus(1))
     relay_v(*row_minus(1))
 
     def key(sign, n, step):
         move = plus if sign > 0 else minus
         return lambda: move(kbuf, ksem, n, (y + step) % YN)
-
-    def attend(row, ok, parts, diagonal=False, steps=None):
-        def run():
-            if steps is None:
-                first = row * YN
-                keys = kbuf[pl.ds(first, YN)].reshape(YN * ROWS, 128)
-                values = jnp.concatenate([vbuf[first + i] for i in range(YN)], axis=1)
-            else:
-                slots = [slot(row, (y + step) % YN) for step in steps]
-                keys = jnp.concatenate([kbuf[s] for s in slots], axis=0)
-                values = jnp.concatenate([vbuf[s] for s in slots], axis=1)
-            all_scores = [dot(keys, qt[part]) for part in parts]
-            for part, scores in zip(parts, all_scores):
-                if diagonal:
-                    key_at = lax.broadcasted_iota(jnp.int32, scores.shape, 0)
-                    query_at = lax.broadcasted_iota(jnp.int32, scores.shape, 1) % ROWS + y * ROWS
-                    scores = jnp.where(query_at >= key_at, scores, -1e30)
-                    new = jnp.max(scores, axis=0, keepdims=True)
-                    weights = jnp.exp(scores - new)
-                    total[part] = jnp.sum(weights, axis=0, keepdims=True)
-                    att[part] = dot(values, weights.astype(BF))
-                else:
-                    old = peak[part]
-                    new = jnp.maximum(old, jnp.max(scores, axis=0, keepdims=True))
-                    weights = jnp.exp(scores - new)
-                    fade = jnp.exp(old - new)
-                    total[part] = total[part] * fade + jnp.sum(weights, axis=0, keepdims=True)
-                    att[part] = att[part] * fade + dot(values, weights.astype(BF))
-                peak[part] = new
-
-        if ok is None:
-            run()
-        else:
-            pl.when(ok)(run)
-
-    fillers = []
-
-    def filler():
-        if fillers:
-            fillers.pop(0)()
-
-    def ready(row, ok, **how):
-        for parts in ((0, 1, 2, 3),) if "steps" in how else ((0, 1), (2, 3)):
-            fillers.append(lambda parts=parts: attend(row, ok, parts, **how))
-
-    def run(*ops):
-        for op in ops:
-            op()
-            filler()
 
     def row_carry():
         for step in (1, 3, 2):
@@ -388,20 +395,15 @@
             all_a = crow[col, 0:1, :] * all_a
         ctot[z, 0:1, :] = all_a
         ctot[z, 1:2, :] = all_s
-        send(ctot.at[z], ctot.at[z], ctsem.at[z], when=has_up, sp=up)
-        send_down(ctot, ctsem, z, goes_down)
-
-    def carry(n):
-        row, ok = row_plus(n)
-        arrived(ctot.at[row], ctsem.at[row], ok)
-        if n < FWD:
-            send(ctot.at[row], ctot.at[row], ctsem.at[row], when=ok & has_up, sp=up)
-        if n <= BACK:
-            row = (z + n) % ZN
-            ok = row <= BACK - 1
-            arrived(ctot.at[row], ctsem.at[row], ok)
-            if n < BACK:
-                send_down(ctot, ctsem, row, ok)
+        pl.semaphore_wait(known.at[2], 1)
+        pl.semaphore_wait(known.at[3], 1)
+        for distance in range(1, ZN):
+            to = ((z + distance) % ZN) * YN + y
+            send(ctot.at[z], ctot.at[z], ctsem.at[z], when=z + distance < ZN, sp=to)
+
+    def carries():
+        for row in range(ZN - 1):
+            arrived(ctot.at[row], ctsem.at[row], row < z)
 
     def fold_total(row, s):
         return ctot[row, 0:1, :] * s + ctot[row, 1:2, :]
@@ -426,37 +428,52 @@
             else:
                 pl.when(when)(lambda copy=copy: copy.wait_send())
 
+    def both(n, *steps):
+        for step in steps:
+            if n <= FWD:
+                key(1, n, step)()
+            if n <= BACK:
+                key(-1, n, step)()
+
+    both(1, 1, 3)
     finish_v(z, always)
-    ready(z, None, diagonal=True)
-    run(key(1, 1, 1), key(-1, 1, 1), key(1, 1, 3), key(-1, 1, 3))
-    run(key(1, 2, 0), key(-1, 2, 0), key(1, 1, 2), key(-1, 1, 2))
-    run(lambda: v_plus(3), lambda: v_minus(3))
-    run(lambda: relay_v(*row_plus(2)), lambda: relay_v(*row_minus(2)), lambda: finish_v(*row_plus(1)))
-    ready(*row_plus(1))
-    run(lambda: finish_v(*row_minus(1)))
-    ready(*row_minus(1))
-    run(row_carry, key(1, 2, 1), key(-1, 2, 1), key(1, 2, 3), key(-1, 2, 3))
-    run(key(1, 3, 0), key(-1, 3, 0), key(1, 2, 2), key(-1, 2, 2))
-    run(lambda: v_plus(4), lambda: relay_v(*row_plus(3)), lambda: relay_v(*row_minus(3)))
-    run(lambda: finish_v(*row_plus(2)))
-    ready(*row_plus(2))
-    run(lambda: carry(1), lambda: finish_v(*row_minus(2)))
-    ready(*row_minus(2))
-    run(key(1, 3, 1), key(-1, 3, 1), lambda: carry(2), key(1, 3, 3), key(-1, 3, 3))
-    run(key(1, 4, 0), key(1, 3, 2), key(-1, 3, 2))
-    run(lambda: relay_v(*row_plus(4)), lambda: finish_v(*row_plus(3)))
-    ready(*row_plus(3))
-    run(lambda: carry(3), lambda: finish_v(*row_minus(3)))
-    ready(*row_minus(3))
-    run(key(1, 4, 1), lambda: carry(4), key(1, 4, 3), drain, lambda: finish_v(*row_plus(4)))
-    fillers.append(recur_output)
+    attend(z, None, steps=(1, 2, 3), earlier=True)
+    both(2, 0)
+    v_plus(3)
+    v_minus(3)
+    both(1, 2)
+    finish_v(*row_plus(1))
+    finish_v(*row_minus(1))
+    relay_v(*row_plus(2))
+    relay_v(*row_minus(2))
+    row_carry()
+    attend(*row_plus(1))
+    both(2, 1, 3)
+    both(3, 0)
+    v_minus(4)
+    attend(*row_minus(1))
+    relay_v(*row_minus(3))
+    both(2, 2)
+    finish_v(*row_plus(2))
+    finish_v(*row_minus(2))
+    attend(*row_plus(2))
+    both(3, 1, 3)
+    both(4, 0)
+    attend(*row_minus(2))
+    both(3, 2)
+    finish_v(*row_plus(3), across=True)
+    finish_v(*row_minus(3))
+    attend(*row_plus(3))
+    both(4, 1, 3)
+    attend(*row_minus(3))
+    drain()
+    carries()
+    recur_output()
     for n in range(4):
-        fillers.append(lambda n=n: recur_project(n))
-    while fillers:
-        filler()
-    key(1, 4, 2)()
-    attend(*row_plus(4), (0, 1), steps=(0, 1, 3, 2))
-    attend(*row_plus(4), (2, 3), steps=(0, 1, 3, 2))
+        recur_project(n)
+    finish_v(*row_minus(4), across=True)
+    both(4, 2)
+    attend(*row_minus(4))
 
     pieces = []
     for h in range(4):
@@ -507,6 +524,7 @@
         vmem((YN, 2, 512), F32), vmem((ZN, 2, 512), F32), vmem((ROWS, 512), F32), vmem((ROWS, 512), F32),
         vmem((4, ROWS, 512), F32), vmem((4, 64, 512), F32), vmem((ROWS, 512), BF),
         dma((24,)), dma((NSEND,)), dma, dma((SP,)), dma((SP,)), dma, dma((YN,)), dma((ZN,)), dma((4,)),
+        pltpu.SemaphoreType.REGULAR((4,)),
     ]
     return pl.pallas_call(
         kernel,

time: 37.8 us -> 34.3 us (0.907)
  the two profiles are of different devices: /device:TPU:193 before, /device:TPU:163 now
where the time goes in v4:
time: 34.3 us; the launch traced here: 34.2 us
  Pallas kernels  33.5 us (98%)
  local copies, waits for them, and re-layouts  0.71 us (2%)
    pallas_call x1, Pallas kernels, body(): pl.pallas_call(kernel, out_shape=pltpu.VMEM((64, D), BF), in_specs=[any_]...  33.5 us
    unnamed x1, local copies, waits for them, and re-layouts  0.71 us

profile of v4, /device:TPU:163, one launch (start us, length us, event | category | flops | bytes accessed | tf_op | source)
XLA Modules:
  0.0 34.2 jit_solution(17335717556387851493)
XLA Ops:
  0.0 33.5 %layer.1 = bf16[64,2048]{1,0:T(8,128)(2,1)S(1)} custom-call(bf16[128,1024]{1,0:T(8,128)(2,1)} %tok_h.1, f32[2,1,1024]{2,1,0:T(1,128)} %bitcast.6, bf16[2048,512]{1,0:T(8,128)(2,1)} %wr_h.1, f32[4,512]{1,0:T(4,128)} %cw_h.1, bf16[8,64,64]{2,1,0:T(8,128)(2,1)} %wgd_h.1, bf16[8,64,64]{2,1,0:T(8,128)(2,1)} %wgi_h.1, f32[1,512]{1,0:T(1,128)} %bitcast.9, ...), custom_call_target="tpu_custom_call" | custom-call | tf_op jit(solution)/shard_map/layer/pallas_call | solution.py:529
  33.5 0.7 %copy.18 = bf16[64,2048]{1,0:T(8,128)(2,1)} copy(bf16[64,2048]{1,0:T(8,128)(2,1)S(1)} %layer.1) | data formatting | bytes 524288

commit v5 on v4

--- a/solution.py
+++ b/solution.py
@@ -1,3 +1,5 @@
+import itertools
+
 import jax
 import jax.numpy as jnp
 from jax import lax
@@ -18,9 +20,9 @@
 SP = ZN * YN
 RATE = 8.0
 EPS = 1e-06
-FWD = 3
-BACK = 4
-NSEND = 144
+FWD = 4
+BACK = 3
+NSEND = 28
 
 
 def dot(a, b):
@@ -37,9 +39,9 @@
 def kernel(
     tok_h, gain_h, wr_h, cw_h, wgd_h, wgi_h, base_h, extra_h, wq_h, wk_h, wv_h, lam_h, hgain_h,
     wor_h, woa_h, ogain_h, out_h,
-    tok, gain, wr, cw, wgd, wgi, base, extra, wq, wkv, lam, hgain, wor, woa, ogain,
+    tok, gain, wall, cw, wgd, wgi, base, extra, lam, hgain, wor, woa, ogain,
     scaled, acc, kbuf, vbuf, rin, halo, xext, qt, att, peak, total, gates,
-    crow, ctot, decs, states, mbuf, mrecv, rout,
+    crow, ctot, decs, states, mbuf, mrecv, mpart, rout,
     lsem, ssem, tsem, ksem, vsem, hsem, crsem, ctsem, msem, known,
 ):
     sp = lax.axis_index("sp")
@@ -47,34 +49,27 @@
     z = sp // YN
     y = sp % YN
 
-    locals_ = []
-
-    def load(src, dst):
-        copy = pltpu.make_async_copy(src, dst, lsem.at[len(locals_)])
-        locals_.append(copy)
-        copy.start()
-        return copy
+    def load(n, *pairs):
+        for src, dst in pairs:
+            pltpu.make_async_copy(src, dst, lsem.at[n]).start()
+
+    def loaded(n, dst):
+        pltpu.make_async_copy(dst, dst, lsem.at[n]).wait()
 
     own_rows = pl.ds(pl.multiple_of(c * HALF, HALF), HALF)
     other_rows = pl.ds(pl.multiple_of((1 - c) * HALF, HALF), HALF)
-    l_tok = load(tok_h, tok.at[c])
-    l_gain = load(gain_h, gain)
-    l_own = [
-        load(wk_h.at[own_rows], wkv.at[own_rows, pl.ds(0, 128)]),
-        load(wv_h.at[own_rows], wkv.at[own_rows, pl.ds(128, 128)]),
-        load(wr_h.at[own_rows], wr.at[own_rows]),
-        load(wq_h.at[own_rows], wq.at[own_rows]),
-    ]
-    l_kv = [
-        load(wk_h.at[other_rows], wkv.at[other_rows, pl.ds(0, 128)]),
-        load(wv_h.at[other_rows], wkv.at[other_rows, pl.ds(128, 128)]),
-    ]
-    l_r = load(wr_h.at[other_rows], wr.at[other_rows])
-    l_q = load(wq_h.at[other_rows], wq.at[other_rows])
-    l_small = [
-        load(cw_h, cw), load(wgd_h, wgd), load(wgi_h, wgi), load(base_h, base), load(extra_h, extra),
-        load(lam_h, lam), load(hgain_h, hgain), load(ogain_h, ogain),
-    ]
+    kv_cols, r_cols, q_cols = pl.ds(0, 256), pl.ds(256, 512), pl.ds(768, 512)
+    load(0, (tok_h, tok.at[c]))
+    load(1, (gain_h, gain))
+
+    def load_kv(n, rows):
+        load(n, (wk_h.at[rows], wall.at[rows, pl.ds(0, 128)]), (wv_h.at[rows], wall.at[rows, pl.ds(128, 128)]))
+
+    load_kv(2, own_rows)
+    load(2, (wr_h.at[own_rows], wall.at[own_rows, r_cols]), (wq_h.at[own_rows], wall.at[own_rows, q_cols]))
+    load_kv(3, other_rows)
+    load(4, (wr_h.at[other_rows], wall.at[other_rows, r_cols]))
+    load(5, (wq_h.at[other_rows], wall.at[other_rows, q_cols]))
 
     barrier = pltpu.get_barrier_semaphore()
     pl.semaphore_signal(barrier, inc=1, device_id={"tp": 1 - c}, device_id_type=MESH)
@@ -101,11 +96,19 @@
         greeted = greeted + when.astype(jnp.int32)
 
     sends = []
-    numbers = iter(range(NSEND))
+    numbers = itertools.count()
+
+    def settle(copy, when):
+        if when is None:
+            copy.wait_send()
+        else:
+            pl.when(when)(lambda: copy.wait_send())
 
     def send(src, dst, rsem, when=None, **target):
+        if len(sends) == NSEND:
+            settle(*sends.pop(0))
         copy = pltpu.make_async_remote_copy(
-            src_ref=src, dst_ref=dst, send_sem=ssem.at[next(numbers)], recv_sem=rsem,
+            src_ref=src, dst_ref=dst, send_sem=ssem.at[next(numbers) % NSEND], recv_sem=rsem,
             device_id=target, device_id_type=MESH,
         )
         sends.append((copy, when))
@@ -135,13 +138,13 @@
             known.at[n], inc=1, device_id={"sp": ((z + distance) % ZN) * YN + y}, device_id_type=MESH
         )
 
-    l_tok.wait()
+    loaded(0, tok.at[c])
     pl.semaphore_wait(barrier, greeted)
     send(tok.at[c], tok.at[c], tsem, tp=1 - c)
-    l_wor = load(wor_h, wor)
-    l_woa = load(woa_h, woa)
-
-    l_gain.wait()
+    load(8, (wor_h, wor))
+    load(9, (woa_h, woa))
+
+    loaded(1, gain)
 
     def scale_half(half):
         x = tok[half].astype(F32)
@@ -151,18 +154,14 @@
     squares = scale_half(c)
     tell(0, 1)
     tell(1, ZN - 1)
-    for copy in l_own:
-        copy.wait()
-    acc[:, 0:256] = dot(scaled[c], wkv[own_rows, :])
-    acc[:, 256:768] = dot(scaled[c], wr[own_rows, :])
-    acc[:, 768:1280] = dot(scaled[c], wq[own_rows, :])
+    loaded(2, wall.at[own_rows])
+    acc[...] = dot(scaled[c], wall[own_rows, :])
 
     arrived(tok.at[1 - c], tsem)
     squares = squares + scale_half(1 - c)
     inverse = lax.rsqrt(squares / D + EPS)
-    for copy in l_kv:
-        copy.wait()
-    kv = (acc[:, 0:256] + dot(scaled[1 - c], wkv[other_rows, :])) * inverse
+    loaded(3, wall.at[other_rows, kv_cols])
+    kv = (acc[:, 0:256] + dot(scaled[1 - c], wall[other_rows, 0:256])) * inverse
     kbuf[sp] = kv[:, 0:128].astype(BF)
     vbuf[sp] = jnp.transpose(kv[:, 128:256]).astype(BF)
 
@@ -178,13 +177,18 @@
     def send_down(buf, sem, at, when):
         send(buf.at[at], buf.at[at], sem.at[at], when=when, sp=down)
 
+    def send_v(row, col, to, kind, when):
+        s = slot(row, col)
+        send(vbuf.at[s], vbuf.at[s], vsem.at[row, kind], when=when, sp=to)
+
     def forward_own(buf, sem, col):
         send_block(buf, sem, z, col, up, has_up)
         send_down(buf, sem, slot(z, col), goes_down)
 
     for step in (1, 3, 2):
         send(kbuf.at[sp], kbuf.at[sp], ksem.at[sp], sp=beside(step))
-    forward_own(vbuf, vsem, y)
+    send_v(z, y, up, 0, has_up)
+    send_v(z, y, down, 0, goes_down)
     forward_own(kbuf, ksem, y)
 
     def plus(buf, sem, d, col):
@@ -212,16 +216,19 @@
 
     def spread_v(row, ok, across=False):
         way = 1 - 2 * (row % 2)
-        send_block(vbuf, vsem, row, y, beside(way), ok)
-        send_block(vbuf, vsem, row, y, beside(-way), ok)
+        send_v(row, y, beside(way), 2 if across else 1, ok)
+        send_v(row, y, beside(-way), 2, ok)
         if across:
-            send_block(vbuf, vsem, row, y, beside(2), ok)
+            send_v(row, y, beside(2), 2, ok)
 
     def relay_v(row, ok):
         way = 1 - 2 * (row % 2)
-        s = slot(row, (y - way + YN) % YN)
-        arrived(vbuf.at[s], vsem.at[s], ok)
-        send(vbuf.at[s], vbuf.at[s], vsem.at[s], when=ok, sp=beside(way))
+        col = (y - way + YN) % YN
+        arrived(vbuf.at[slot(row, col)], vsem.at[row, 1], ok)
+        send_v(row, col, beside(way), 2, ok)
+
+    def finish_v(row, ok, across=False):
+        arrived(vbuf.at[pl.ds(slot(row, 0), 3 if across else 2)], vsem.at[row, 2], ok)
 
     def keys_beside():
         for step in (1, 3):
@@ -236,35 +243,39 @@
         arrived(kbuf.at[s], ksem.at[s])
         forward_own(kbuf, ksem, col)
 
-    def finish_v(row, ok, across=False):
-        way = 1 - 2 * (row % 2)
-        cols = [(y + way + YN) % YN, (y + 2) % YN]
-        if across:
-            cols.append((y - way + YN) % YN)
-        for col in cols:
-            s = slot(row, col)
-            arrived(vbuf.at[s], vsem.at[s], ok)
-
     always = z >= 0
     spread_v(z, always)
 
-    l_r.wait()
-    recur = ((acc[:, 256:768] + dot(scaled[1 - c], wr[other_rows, :])) * inverse).astype(BF)
+    loaded(4, wall.at[other_rows, r_cols])
+    recur = ((acc[:, 256:768] + dot(scaled[1 - c], wall[other_rows, 256:768])) * inverse).astype(BF)
     rin[...] = recur
     send(rin.at[pl.ds(ROWS - 16, 16)], halo, hsem, when=sp < SP - 1, sp=(sp + 1) % SP)
     xext[pl.ds(8, ROWS), :] = recur.astype(F32)
 
 
     def v_plus(d):
-        plus(vbuf, vsem, d, y)
-        spread_v(*row_plus(d), across=d == FWD)
+        row, ok = row_plus(d)
+        arrived(vbuf.at[slot(row, y)], vsem.at[row, 0], ok)
+        if d < FWD:
+            send_v(row, y, up, 0, ok & has_up)
+        spread_v(row, ok, across=d == FWD)
 
     def v_minus(e):
-        minus(vbuf, vsem, e, y)
+        row = (z + e) % ZN
+        ok = row <= BACK - 1
+        arrived(vbuf.at[slot(row, y)], vsem.at[row, 0], ok)
+        if e < BACK:
+            send_v(row, y, down, 0, ok)
         spread_v(*row_minus(e), across=e == BACK)
 
-    l_q.wait()
-    query = ((acc[:, 768:1280] + dot(scaled[1 - c], wq[other_rows, :])) * inverse).astype(BF)
+    loaded(5, wall.at[other_rows, q_cols])
+    small = (
+        (cw_h, cw), (wgd_h, wgd), (wgi_h, wgi), (base_h, base), (extra_h, extra), (lam_h, lam),
+        (hgain_h, hgain), (ogain_h, ogain),
+    )
+    for n, pair in enumerate(small):
+        load(n, pair)
+    query = ((acc[:, 768:1280] + dot(scaled[1 - c], wall[other_rows, 768:1280])) * inverse).astype(BF)
     query = query.astype(F32) * HEAD ** (-0.5)
     qt[...] = jnp.zeros_like(qt)
     for h in range(4):
@@ -328,8 +339,8 @@
     tell(2, 2)
     tell(3, ZN - 2)
 
-    for copy in l_small:
-        copy.wait()
+    for n, (_, dst) in enumerate(small):
+        loaded(n, dst)
     arrived(halo, hsem, sp > 0)
     before = halo[8:16, :].astype(F32)
     xext[pl.ds(0, 8), :] = jnp.where(sp > 0, before, 0.0)
@@ -368,26 +379,12 @@
         crow[y, 1:2, cols] = b[ROWS - 1 : ROWS]
 
 
-    recur_columns(0)
-    recur_columns(1)
-    keys_across()
-    v_plus(2)
-    v_minus(2)
-    recur_columns(2)
-    recur_columns(3)
-    for step in (1, 3, 2):
-        send(crow.at[y], crow.at[y], crsem.at[y], sp=beside(step))
-    relay_v(*row_plus(1))
-    relay_v(*row_minus(1))
-
     def key(sign, n, step):
         move = plus if sign > 0 else minus
         return lambda: move(kbuf, ksem, n, (y + step) % YN)
 
     def row_carry():
-        for step in (1, 3, 2):
-            col = (y + step) % YN
-            arrived(crow.at[col], crsem.at[col])
+        arrived(crow.at[pl.ds(0, YN - 1)], crsem)
         all_a = crow[0, 0:1, :]
         all_s = crow[0, 1:2, :]
         for col in range(1, YN):
@@ -399,11 +396,10 @@
         pl.semaphore_wait(known.at[3], 1)
         for distance in range(1, ZN):
             to = ((z + distance) % ZN) * YN + y
-            send(ctot.at[z], ctot.at[z], ctsem.at[z], when=z + distance < ZN, sp=to)
+            send(ctot.at[z], ctot.at[z], ctsem, sp=to)
 
     def carries():
-        for row in range(ZN - 1):
-            arrived(ctot.at[row], ctsem.at[row], row < z)
+        arrived(ctot.at[pl.ds(0, ZN - 1)], ctsem)
 
     def fold_total(row, s):
         return ctot[row, 0:1, :] * s + ctot[row, 1:2, :]
@@ -415,18 +411,14 @@
         carry_in = lax.fori_loop(0, z, fold_total, jnp.zeros((1, 512), F32))
         carry_in = lax.fori_loop(0, y, fold_row, carry_in)
         rout[...] = (states[...] + decs[...] * carry_in).astype(BF)
-        l_wor.wait()
+        loaded(8, wor)
 
     def recur_project(n):
         mbuf[n] = dot(rout[...], wor[:, n * 512 : n * 512 + 512])
 
     def drain():
         while sends:
-            copy, when = sends.pop(0)
-            if when is None:
-                copy.wait_send()
-            else:
-                pl.when(when)(lambda copy=copy: copy.wait_send())
+            settle(*sends.pop(0))
 
     def both(n, *steps):
         for step in steps:
@@ -435,45 +427,61 @@
             if n <= BACK:
                 key(-1, n, step)()
 
+    def relay(n):
+        if n < FWD:
+            relay_v(*row_plus(n))
+        if n < BACK:
+            relay_v(*row_minus(n))
+
+    def finish(sign, n):
+        row_of, most = (row_plus, FWD) if sign > 0 else (row_minus, BACK)
+        finish_v(*row_of(n), across=n == most)
+        attend(*row_of(n))
+
+    far = 1 if FWD == 4 else -1
+
+    recur_columns(0)
+    recur_columns(1)
+    keys_across()
+    v_plus(2)
+    v_minus(2)
+    relay(1)
+    recur_columns(2)
+    both(2, 0)
+    recur_columns(3)
+    for step in (1, 3, 2):
+        send(crow.at[y], crow.at[y], crsem, sp=beside(step))
     both(1, 1, 3)
     finish_v(z, always)
     attend(z, None, steps=(1, 2, 3), earlier=True)
-    both(2, 0)
+    both(1, 2)
     v_plus(3)
     v_minus(3)
-    both(1, 2)
-    finish_v(*row_plus(1))
-    finish_v(*row_minus(1))
-    relay_v(*row_plus(2))
-    relay_v(*row_minus(2))
+    relay(2)
+    finish(1, 1)
     row_carry()
-    attend(*row_plus(1))
+    both(3, 0)
     both(2, 1, 3)
-    both(3, 0)
-    v_minus(4)
-    attend(*row_minus(1))
-    relay_v(*row_minus(3))
+    finish(-1, 1)
     both(2, 2)
-    finish_v(*row_plus(2))
-    finish_v(*row_minus(2))
-    attend(*row_plus(2))
+    (v_plus if FWD == 4 else v_minus)(4)
+    relay(3)
+    finish(1, 2)
     both(3, 1, 3)
     both(4, 0)
-    attend(*row_minus(2))
+    finish(-1, 2)
     both(3, 2)
-    finish_v(*row_plus(3), across=True)
-    finish_v(*row_minus(3))
-    attend(*row_plus(3))
-    both(4, 1, 3)
-    attend(*row_minus(3))
-    drain()
+    finish(-far, 3)
     carries()
     recur_output()
     for n in range(4):
         recur_project(n)
-    finish_v(*row_minus(4), across=True)
+    finish(far, 3)
+    both(4, 1, 3)
     both(4, 2)
-    attend(*row_minus(4))
+    while len(sends) > 8:
+        settle(*sends.pop(0))
+    finish(far, 4)
 
     pieces = []
     for h in range(4):
@@ -487,20 +495,21 @@
 
     mine = pl.ds(pl.multiple_of(c * 64, 64), 64)
     theirs = pl.ds(pl.multiple_of((1 - c) * 64, 64), 64)
-    l_woa.wait()
+    loaded(9, woa)
     for n in range(4):
         mbuf[n] += dot(attend_out, woa[:, n * 512 : n * 512 + 512])
-        send(mbuf.at[n, theirs], mrecv.at[n], msem.at[n], tp=1 - c)
+        mpart[n] = mbuf[n, theirs, :].astype(BF)
+        send(mpart.at[n], mrecv.at[n], msem.at[n], tp=1 - c)
     power = jnp.zeros((64, 1), F32)
     for n in range(4):
         arrived(mrecv.at[n], msem.at[n])
-        whole = mbuf[n, mine, :] + mrecv[n]
-        mrecv[n] = whole
+        whole = mbuf[n, mine, :] + mrecv[n].astype(F32)
+        mbuf[n, mine, :] = whole
         power = power + jnp.sum(whole * whole, axis=1, keepdims=True)
     scale = lax.rsqrt(power / D + EPS)
     for n in range(4):
         cols = slice(n * 512, n * 512 + 512)
-        out_h[:, cols] = (mrecv[n] * scale * ogain[:, cols]).astype(BF)
+        out_h[:, cols] = (mbuf[n, mine, :] * scale * ogain[:, cols]).astype(BF)
     drain()
 
 
@@ -512,9 +521,9 @@
     vmem = pltpu.VMEM
     dma = pltpu.SemaphoreType.DMA
     scratch = [
-        vmem((2, ROWS, HALF), BF), vmem((2, 1, HALF), F32), vmem((D, 512), BF), vmem((4, 512), F32),
+        vmem((2, ROWS, HALF), BF), vmem((2, 1, HALF), F32), vmem((D, 1280), BF), vmem((4, 512), F32),
         vmem((8, 64, 64), BF), vmem((8, 64, 64), BF), vmem((1, 512), F32), vmem((8, ROWS), F32),
-        vmem((D, 512), BF), vmem((D, 256), BF), vmem((1, 4), F32), vmem((1, 128), F32),
+        vmem((1, 4), F32), vmem((1, 128), F32),
         vmem((512, D), BF), vmem((512, D), BF), vmem((1, D), F32),
         vmem((2, ROWS, HALF), BF), vmem((ROWS, 1280), F32),
         vmem((SP, ROWS, 128), BF), vmem((SP, 128, ROWS), BF),
@@ -522,8 +531,8 @@
         vmem((4, 128, 256), BF), vmem((4, 128, 256), F32), vmem((4, 1, 256), F32), vmem((4, 1, 256), F32),
         vmem((4, 128, 256), BF),
         vmem((YN, 2, 512), F32), vmem((ZN, 2, 512), F32), vmem((ROWS, 512), F32), vmem((ROWS, 512), F32),
-        vmem((4, ROWS, 512), F32), vmem((4, 64, 512), F32), vmem((ROWS, 512), BF),
-        dma((24,)), dma((NSEND,)), dma, dma((SP,)), dma((SP,)), dma, dma((YN,)), dma((ZN,)), dma((4,)),
+        vmem((4, ROWS, 512), F32), vmem((4, 64, 512), BF), vmem((4, 64, 512), BF), vmem((ROWS, 512), BF),
+        dma((10,)), dma((NSEND,)), dma, dma((SP,)), dma((ZN, 3)), dma, dma, dma, dma((4,)),
         pltpu.SemaphoreType.REGULAR((4,)),
     ]
     return pl.pallas_call(

time: 34.3 us -> 31.6 us (0.921)
  the two profiles are of different devices: /device:TPU:163 before, /device:TPU:1 now
where the time goes in v5:
time: 31.6 us; the launch traced here: 31.5 us
  Pallas kernels  30.8 us (97%)
  local copies, waits for them, and re-layouts  0.71 us (2%)
    pallas_call x1, Pallas kernels, body(): pl.pallas_call(kernel, out_shape=pltpu.VMEM((64, D), BF), in_specs=[any_]...  30.8 us
    unnamed x1, local copies, waits for them, and re-layouts  0.71 us

profile of v5, /device:TPU:1, one launch (start us, length us, event | category | flops | bytes accessed | tf_op | source)
XLA Modules:
  0.0 31.5 jit_solution(12970686988888863434)
XLA Ops:
  0.0 30.8 %layer.1 = bf16[64,2048]{1,0:T(8,128)(2,1)S(1)} custom-call(bf16[128,1024]{1,0:T(8,128)(2,1)} %tok_h.1, f32[2,1,1024]{2,1,0:T(1,128)} %bitcast.6, bf16[2048,512]{1,0:T(8,128)(2,1)} %wr_h.1, f32[4,512]{1,0:T(4,128)} %cw_h.1, bf16[8,64,64]{2,1,0:T(8,128)(2,1)} %wgd_h.1, bf16[8,64,64]{2,1,0:T(8,128)(2,1)} %wgi_h.1, f32[1,512]{1,0:T(1,128)} %bitcast.9, ...), custom_call_target="tpu_custom_call" | custom-call | tf_op jit(solution)/shard_map/layer/pallas_call | solution.py:538
  30.8 0.7 %copy.18 = bf16[64,2048]{1,0:T(8,128)(2,1)} copy(bf16[64,2048]{1,0:T(8,128)(2,1)S(1)} %layer.1) | data formatting | bytes 524288

commit v6 on v5

--- a/solution.py
+++ b/solution.py
@@ -21,6 +21,8 @@
 RATE = 8.0
 EPS = 1e-06
 FWD = 4
+STRAIGHT_UP = (1, 2, 4)
+STRAIGHT_DOWN = (3,)
 BACK = 3
 NSEND = 28
 
@@ -258,7 +260,7 @@
         arrived(vbuf.at[slot(row, y)], vsem.at[row, 0], ok)
         if d < FWD:
             send_v(row, y, up, 0, ok & has_up)
-        spread_v(row, ok, across=d == FWD)
+        spread_v(row, ok, across=d in STRAIGHT_UP)
 
     def v_minus(e):
         row = (z + e) % ZN
@@ -266,7 +268,7 @@
         arrived(vbuf.at[slot(row, y)], vsem.at[row, 0], ok)
         if e < BACK:
             send_v(row, y, down, 0, ok)
-        spread_v(*row_minus(e), across=e == BACK)
+        spread_v(*row_minus(e), across=e in STRAIGHT_DOWN)
 
     loaded(5, wall.at[other_rows, q_cols])
     small = (
@@ -396,10 +398,11 @@
         pl.semaphore_wait(known.at[3], 1)
         for distance in range(1, ZN):
             to = ((z + distance) % ZN) * YN + y
-            send(ctot.at[z], ctot.at[z], ctsem, sp=to)
+            send(ctot.at[z], ctot.at[z], ctsem.at[jnp.minimum(z, ZN - 2)], when=z + distance < ZN, sp=to)
 
     def carries():
-        arrived(ctot.at[pl.ds(0, ZN - 1)], ctsem)
+        for row in range(ZN - 1):
+            arrived(ctot.at[row], ctsem.at[row], row < z)
 
     def fold_total(row, s):
         return ctot[row, 0:1, :] * s + ctot[row, 1:2, :]
@@ -428,14 +431,14 @@
                 key(-1, n, step)()
 
     def relay(n):
-        if n < FWD:
+        if n not in STRAIGHT_UP:
             relay_v(*row_plus(n))
-        if n < BACK:
+        if n not in STRAIGHT_DOWN:
             relay_v(*row_minus(n))
 
     def finish(sign, n):
-        row_of, most = (row_plus, FWD) if sign > 0 else (row_minus, BACK)
-        finish_v(*row_of(n), across=n == most)
+        row_of, straight = (row_plus, STRAIGHT_UP) if sign > 0 else (row_minus, STRAIGHT_DOWN)
+        finish_v(*row_of(n), across=n in straight)
         attend(*row_of(n))
 
     far = 1 if FWD == 4 else -1
@@ -445,15 +448,15 @@
     keys_across()
     v_plus(2)
     v_minus(2)
+    recur_columns(2)
     relay(1)
-    recur_columns(2)
-    both(2, 0)
     recur_columns(3)
     for step in (1, 3, 2):
         send(crow.at[y], crow.at[y], crsem, sp=beside(step))
     both(1, 1, 3)
     finish_v(z, always)
     attend(z, None, steps=(1, 2, 3), earlier=True)
+    both(2, 0)
     both(1, 2)
     v_plus(3)
     v_minus(3)
@@ -532,7 +535,7 @@
         vmem((4, 128, 256), BF),
         vmem((YN, 2, 512), F32), vmem((ZN, 2, 512), F32), vmem((ROWS, 512), F32), vmem((ROWS, 512), F32),
         vmem((4, ROWS, 512), F32), vmem((4, 64, 512), BF), vmem((4, 64, 512), BF), vmem((ROWS, 512), BF),
-        dma((10,)), dma((NSEND,)), dma, dma((SP,)), dma((ZN, 3)), dma, dma, dma, dma((4,)),
+        dma((10,)), dma((NSEND,)), dma, dma((SP,)), dma((ZN, 3)), dma, dma, dma((ZN - 1,)), dma((4,)),
         pltpu.SemaphoreType.REGULAR((4,)),
     ]
     return pl.pallas_call(

time: 31.6 us -> 30.4 us (0.962)
  the two profiles are of different devices: /device:TPU:1 before, /device:TPU:193 now
where the time goes in v6:
time: 30.4 us; the launch traced here: 30 us
  Pallas kernels  29.3 us (96%)
  local copies, waits for them, and re-layouts  0.71 us (2%)
    pallas_call x1, Pallas kernels, body(): pl.pallas_call(kernel, out_shape=pltpu.VMEM((64, D), BF), in_specs=[any_]...  29.3 us
    unnamed x1, local copies, waits for them, and re-layouts  0.71 us

profile of v6, /device:TPU:193, one launch (start us, length us, event | category | flops | bytes accessed | tf_op | source)
XLA Modules:
  0.0 30.0 jit_solution(2433386189247806382)
XLA Ops:
  0.0 29.3 %layer.1 = bf16[64,2048]{1,0:T(8,128)(2,1)S(1)} custom-call(bf16[128,1024]{1,0:T(8,128)(2,1)} %tok_h.1, f32[2,1,1024]{2,1,0:T(1,128)} %bitcast.6, bf16[2048,512]{1,0:T(8,128)(2,1)} %wr_h.1, f32[4,512]{1,0:T(4,128)} %cw_h.1, bf16[8,64,64]{2,1,0:T(8,128)(2,1)} %wgd_h.1, bf16[8,64,64]{2,1,0:T(8,128)(2,1)} %wgi_h.1, f32[1,512]{1,0:T(1,128)} %bitcast.9, ...), custom_call_target="tpu_custom_call" | custom-call | tf_op jit(solution)/shard_map/layer/pallas_call | solution.py:541
  29.3 0.7 %copy.18 = bf16[64,2048]{1,0:T(8,128)(2,1)} copy(bf16[64,2048]{1,0:T(8,128)(2,1)S(1)} %layer.1) | data formatting | bytes 524288
